TPU v7x, 32 devices: a whole 2x2x4 slice. The times are simulated.
32 devices in a mesh: sp: 8 (over z, core), tp: 4 (over y, x).
Axes of the slice: x: 2, y: 2, z: 4, core: 2. Of those that a mesh axis runs over, the one named last changes fastest.
Arguments:
- queries: bfloat16 [4096, 1024], P('sp', 'tp'), may hold values from -20 to 20
- key_vectors: bfloat16 [4096, 1024], P('sp', 'tp'), may hold values from -20 to 20
- value_vectors: bfloat16 [4096, 1024], P('sp', 'tp'), may hold values from -6 to 6
- log_gate_sums: float32 [4096, 16], P('sp', 'tp'), may hold values from -588 to 0, as said below
- residual: bfloat16 [4096, 2048], P('sp', 'tp'), may hold values from -24 to 24
- out_weight: bfloat16 [1024, 2048], P(None, 'tp'), may hold values from -0.75 to 0.75
- norm_gain: bfloat16 [2048], replicated, may hold values from 0.099609375 to 1.8984375
- routes: int32 [4096, 2], P('sp'), may hold values from 0 to 31, all different within a row; in each aligned block of 512 rows (0 to 511, 512 to 1023, ...) at most 40 rows name the same one
- route_weight: float32 [4096, 2], P('sp'), may hold values from 0.5 to 1.5
- expert_gate: bfloat16 [32, 2048, 512], P('sp', None, 'tp'), may hold values from -0.125 to 0.125
- expert_up: bfloat16 [32, 2048, 512], P('sp', None, 'tp'), may hold values from -0.125 to 0.125
- expert_down: bfloat16 [32, 512, 2048], P('sp', None, 'tp'), may hold values from -0.25 to 0.25
- shared_gate: bfloat16 [2048, 512], P(None, 'tp'), may hold values from -0.125 to 0.125
- shared_up: bfloat16 [2048, 512], P(None, 'tp'), may hold values from -0.125 to 0.125
- shared_down: bfloat16 [512, 2048], P(None, 'tp'), may hold values from -0.25 to 0.25
Outputs:
- layer_out: bfloat16 [4096, 2048], P('sp', 'tp')
Inputs may be any that keep to these rules, and one draw needn't show every extreme that they name: `log_gate_sums`: for each head the values do not rise along the positions. `routes`: each row names 2 different experts; among the rows of one index of sp no expert is named by more than 40 rows, a bound that some block reaches.
All inputs are finite; a program needn't handle non-finite values.
Results may differ from a plain program's by a relative error of at most 0.014.
Values may be sent and summed in bfloat16 or wider, within the bound.
No kernel may reach another device: no remote copies, remote signals or barrier semaphores. Data moves between devices by JAX's collectives and lax.ppermute only.
A program may use at most 64 MiB of HBM per device.

v0:
```python
import functools
import math

import jax
import jax.numpy as jnp
from jax import lax
from jax.experimental import pallas as pl
from jax.experimental.pallas import tpu as pltpu
from jax.sharding import PartitionSpec as P


HDIM = 64
EPSILON = 1e-06
LOG2E = math.log2(math.e)
LOW = -1e30
F32 = jnp.float32
BF16 = jnp.bfloat16


def silu_gate(gate_part, up_part):
    return jax.nn.silu(gate_part) * up_part


def call(kernel, out_shape, args, smem=0, scratch=()):
    vm = pl.BlockSpec(memory_space=pltpu.VMEM)
    sm = pl.BlockSpec(memory_space=pltpu.SMEM)
    single = not isinstance(out_shape, (list, tuple))
    return pl.pallas_call(
        kernel,
        out_shape=out_shape,
        in_specs=[sm] * smem + [vm] * (len(args) - smem),
        out_specs=vm if single else [vm] * len(out_shape),
        scratch_shapes=list(scratch),
    )(*args)


def low_lanes(shape):
    return lax.broadcasted_iota(jnp.int32, shape, 1) < HDIM


def swap_halves(x):
    return pltpu.roll(x, HDIM, 1)


def pack_kernel(heads, z_ref, q_ref, k_ref, v_ref, g_ref, *slabs):
    tok = q_ref.shape[0]
    half = tok // 2
    low = low_lanes((tok, 2 * HDIM))
    low_half = low_lanes((half, 2 * HDIM))
    o_ref = slabs[-1]
    slabs = slabs[:-1]
    gates = g_ref[...]
    for pair in range(heads // 2):
        cols = slice(pair * 2 * HDIM, (pair + 1) * 2 * HDIM)
        q = q_ref[:, cols].astype(F32)
        k = k_ref[:, cols].astype(F32)
        v = v_ref[:, cols].astype(F32)
        o_ref[2 * pair, 0:tok] = jnp.where(low, k, swap_halves(v)).astype(BF16)
        o_ref[2 * pair + 1, 0:tok] = jnp.where(low, swap_halves(k), v).astype(BF16)
        qa, qb = q[:half], q[half:]
        o_ref[2 * pair, tok : tok + half] = jnp.where(low_half, qa, swap_halves(qb)).astype(BF16)
        o_ref[2 * pair + 1, tok : tok + half] = jnp.where(low_half, swap_halves(qa), qb).astype(BF16)
    rows = tok // 128
    for h in range(heads):
        left = gates[h : h + 1]
        pieces = []
        for _ in range(3):
            piece = left.astype(BF16).astype(F32)
            left = left - piece
            pieces += [piece[:, r * 128 : (r + 1) * 128] for r in range(rows)]
        pad = o_ref.shape[1] - tok - half - len(pieces)
        pieces.append(jnp.zeros((pad, 128), F32))
        o_ref[h, tok + half :] = jnp.concatenate(pieces, axis=0).astype(BF16)
    for i, slab in enumerate(slabs):
        slab[...] = o_ref[z_ref[0] ^ i]


def attn_kernel(nz, tok, c_ref, z_ref, *refs):
    owns, sws, outs = refs[:nz], refs[nz : 2 * nz], refs[2 * nz : 3 * nz]
    kv_scr, vo_scr, g_scr, q_scr, o_scr = refs[3 * nz :]
    core = c_ref[0]
    half = tok // 2
    wide = 2 * tok
    rows = tok // 128
    low_tok = low_lanes((tok, 128))
    low_half = low_lanes((half, 128))
    for i in range(nz):
        z = z_ref[0] ^ i
        q_scr[z] = owns[i][tok : tok + half]
        for ref, at in ((owns[i], core), (sws[i], 1 - core)):
            kv = ref[0:tok]
            spot = pl.ds(pl.multiple_of(at * tok, tok), tok)
            kv_scr[z, spot] = kv
            vo_scr[z, spot] = jnp.where(low_tok, 1.0, kv.astype(F32)).astype(BF16)
            g = ref[tok + half :].astype(F32)
            g = (g[0:rows] + g[rows : 2 * rows] + g[2 * rows : 3 * rows]) * LOG2E
            g = jnp.concatenate([g[r : r + 1] for r in range(rows)], axis=1)
            g_scr[z, 0:1, spot] = g
    scale = HDIM ** (-0.5) * LOG2E

    def step(q, z, state, mask=None):
        m, acc = state
        s = lax.dot_general(q, kv_scr[z], (((1,), (1,)), ((), ())), preferred_element_type=F32)
        t = s * scale - g_scr[z, 0:1]
        if mask is not None:
            t = jnp.where(mask, t, LOW)
        top = jnp.maximum(m, jnp.max(t, axis=1, keepdims=True))
        p = jnp.exp2(t - top)
        acc = acc * jnp.exp2(m - top) + jnp.dot(p.astype(BF16), vo_scr[z], preferred_element_type=F32)
        return top, acc

    key_at = lax.broadcasted_iota(jnp.int32, (half, wide), 1)
    row_at = lax.broadcasted_iota(jnp.int32, (half, wide), 0) + core * tok

    def one_block(zq, carry):
        packed = q_scr[zq].astype(F32)
        qs = (
            jnp.where(low_half, packed, 0.0).astype(BF16),
            jnp.where(low_half, swap_halves(packed), 0.0).astype(BF16),
        )
        start = tuple((jnp.full((half, 1), LOW, F32), jnp.zeros((half, 128), F32)) for _ in qs)
        state = lax.fori_loop(0, zq, lambda z, st: tuple(step(q, z, s) for q, s in zip(qs, st)), start)
        state = tuple(
            step(q, zq, s, key_at <= row_at + i * half) for i, (q, s) in enumerate(zip(qs, state))
        )
        acc_a, acc_b = state[0][1], state[1][1]
        out_a = swap_halves(acc_a) / acc_a
        out_b = acc_b / swap_halves(acc_b)
        o_scr[zq] = jnp.where(low_half, out_a, out_b).astype(BF16)
        return carry

    lax.fori_loop(0, nz, one_block, 0)
    for i in range(nz):
        outs[i][...] = o_scr[z_ref[0] ^ i]


def route_kernel(experts, cap, rt_ref, d_ref, c0_ref, c1_ref):
    tok = rt_ref.shape[1]
    slots = experts * cap
    at = lax.broadcasted_iota(jnp.int32, (tok, tok), 0)
    bt = lax.broadcasted_iota(jnp.int32, (tok, tok), 1)
    eid = lax.broadcasted_iota(jnp.int32, (experts, tok), 0)
    hot = [jnp.where(eid == rt_ref[k : k + 1], 1.0, 0.0) for k in range(2)]
    before = jnp.where(at < bt, 1.0, 0.0).astype(BF16)
    rank = jnp.dot((hot[0] + hot[1]).astype(BF16), before, preferred_element_type=F32)
    place = rank + (eid * cap).astype(F32)
    rows = [jnp.sum(h * place, axis=0, keepdims=True).astype(jnp.int32) for h in hot]
    sid = lax.broadcasted_iota(jnp.int32, (slots, tok), 0)
    d_ref[...] = jnp.where((sid == rows[0]) | (sid == rows[1]), 1.0, 0.0).astype(BF16)
    cols = jnp.concatenate([r.astype(F32) for r in rows] * 4, axis=0).T.astype(jnp.int32)
    cols = [cols[:, k : k + 1] for k in range(2)]
    sid = lax.broadcasted_iota(jnp.int32, (tok, slots), 1)
    c0_ref[...] = jnp.where(sid == cols[0], 1.0, 0.0).astype(BF16)
    c1_ref[...] = jnp.where(sid == cols[1], 1.0, 0.0).astype(BF16)


def mid_kernel(heads, cap, t_ref, z_ref, *refs):
    n = len(refs) - 5
    parts, (w_ref, r_ref, d_ref, m_ref, out_ref) = refs[:n], refs[n:]
    half = parts[0].shape[1]
    width = heads * HDIM
    low = low_lanes((half, 2 * HDIM))
    tops = [None, None]
    for k in range(n):
        src = t_ref[0] ^ k
        w = w_ref[pl.ds(pl.multiple_of(src * width, width), width), :]
        ab = ([], [])
        for pair in range(heads // 2):
            p0 = parts[k][z_ref[0] ^ (2 * pair)].astype(F32)
            p1 = parts[k][z_ref[0] ^ (2 * pair + 1)].astype(F32)
            ab[0].append(jnp.where(low, p0, swap_halves(p1)).astype(BF16))
            ab[1].append(jnp.where(low, swap_halves(p0), p1).astype(BF16))
        for i in range(2):
            got = jnp.dot(jnp.concatenate(ab[i], axis=1), w, preferred_element_type=F32)
            tops[i] = got if tops[i] is None else tops[i] + got
    for i in range(2):
        rows = slice(i * half, (i + 1) * half)
        m_ref[rows] = (r_ref[rows].astype(F32) + tops[i]).astype(BF16)
    mid = m_ref[...]
    experts = out_ref.shape[0]
    group = 4
    for e in range(0, experts, group):
        got = jnp.dot(d_ref[e * cap : (e + group) * cap], mid, preferred_element_type=F32)
        for i in range(group):
            out_ref[e + i] = got[i * cap : (i + 1) * cap].astype(BF16)


def normed_of(parts, gains, width):
    total = None
    for x in parts:
        sq = jnp.sum(x * x, axis=1, keepdims=True)
        total = sq if total is None else total + sq
    inverse = lax.rsqrt(total / width + EPSILON)
    return [(x * inverse * g).astype(BF16) for x, g in zip(parts, gains)]


def shared_kernel(t_ref, *refs):
    n = len(refs) - 4
    parts, (gain_ref, gate_ref, up_ref, o_ref) = refs[:n], refs[n:]
    part_width = parts[0].shape[1]
    width = n * part_width
    srcs = [t_ref[0] ^ k for k in range(n)]
    normed = normed_of([p[...].astype(F32) for p in parts], [gain_ref[s] for s in srcs], width)
    both = None
    for s, x in zip(srcs, normed):
        rows = pl.ds(pl.multiple_of(s * part_width, part_width), part_width)
        w = jnp.concatenate([gate_ref[rows, :], up_ref[rows, :]], axis=1)
        got = jnp.dot(x, w, preferred_element_type=F32)
        both = got if both is None else both + got
    hid = gate_ref.shape[1]
    o_ref[...] = silu_gate(both[:, :hid], both[:, hid:]).astype(BF16)


def expert_kernel(sp, tp, t_ref, x_ref, gain_ref, *refs):
    pairs, downs = refs[:tp], refs[tp : 2 * tp]
    y_ref, x_scr, h_scr = refs[2 * tp :]
    me = t_ref[0]
    cap, part_width = x_ref.shape[1:]
    parts = [
        jnp.concatenate([x_ref[s * tp + t].astype(F32) for s in range(sp)], axis=0) for t in range(tp)
    ]
    normed = normed_of(parts, [gain_ref[t] for t in range(tp)], tp * part_width)
    for t in range(tp):
        x_scr[:, t * part_width : (t + 1) * part_width] = normed[t]
    x = x_scr[...]
    hid = pairs[0].shape[1] // 2
    for k in range(tp):
        both = jnp.dot(x, pairs[k][...], preferred_element_type=F32)
        spot = pl.ds(pl.multiple_of((me ^ k) * hid, hid), hid)
        h_scr[:, spot] = silu_gate(both[:, :hid], both[:, hid:]).astype(BF16)
    h = h_scr[...]
    for k in range(tp):
        y = jnp.dot(h, downs[k][...], preferred_element_type=F32)
        for s in range(sp):
            y_ref[s * tp + (me ^ k)] = y[s * cap : (s + 1) * cap].astype(BF16)


def final_kernel(t_ref, *refs):
    n = len(refs) - 8
    hids = refs[:n]
    down_ref, mid_ref, ret_ref, c0_ref, c1_ref, w_ref, o_ref, h_scr = refs[n:]
    hid = hids[0].shape[1]
    for k in range(n):
        spot = pl.ds(pl.multiple_of((t_ref[0] ^ k) * hid, hid), hid)
        h_scr[:, spot] = hids[k][...]
    out = jnp.dot(h_scr[...], down_ref[...], preferred_element_type=F32)
    experts, cap, width = ret_ref.shape
    rows = ret_ref[...].astype(F32).reshape(experts * cap, width).astype(BF16)
    out = out + mid_ref[...].astype(F32)
    w = jnp.concatenate([w_ref[...]] * 4, axis=0).T
    out = out + w[:, 0:1] * jnp.dot(c0_ref[...], rows, preferred_element_type=F32)
    out = out + w[:, 1:2] * jnp.dot(c1_ref[...], rows, preferred_element_type=F32)
    o_ref[...] = out.astype(BF16)


def shards(
    queries,
    key_vectors,
    value_vectors,
    log_gate_sums,
    residual,
    out_weight,
    norm_gain,
    routes,
    route_weight,
    expert_gate,
    expert_up,
    expert_down,
    shared_gate,
    shared_up,
    shared_down,
):
    sp, tp = lax.axis_size("sp"), lax.axis_size("tp")
    tok = queries.shape[0]
    heads = log_gate_sums.shape[1]
    width = residual.shape[1]
    exp_dev = expert_gate.shape[0]
    experts = exp_dev * sp
    top_count = routes.shape[1]
    cap = 5 * tok * top_count // (4 * experts)
    nz = sp // 2
    me = lax.axis_index("tp")
    me_ref = me.astype(jnp.int32).reshape(1)
    core_ref = (lax.axis_index("sp") % 2).astype(jnp.int32).reshape(1)
    half = tok // 2
    rows = tok + half + -(-3 * (tok // 128) // 16) * 16

    def over_tp(x, k):
        return lax.ppermute(x, "tp", [(i, i ^ k) for i in range(tp)])

    def all_tp(x):
        return [x] + [over_tp(x, k) for k in range(1, tp)]

    z = lax.axis_index("sp") // 2
    z_ref = z.astype(jnp.int32).reshape(1)

    def over_z(x, k):
        return lax.ppermute(x, "sp", [(i, i ^ (2 * k)) for i in range(sp)])

    slabs = call(
        functools.partial(pack_kernel, heads),
        [jax.ShapeDtypeStruct((rows, 128), BF16)] * heads,
        (z_ref, queries, key_vectors, value_vectors, log_gate_sums.T),
        smem=1,
        scratch=(pltpu.VMEM((heads, rows, 128), BF16),),
    )
    owns = [slabs[0]] + [over_z(slabs[k], k) for k in range(1, nz)]
    swapped = [lax.ppermute(x, "sp", [(i, i ^ 1) for i in range(sp)]) for x in owns]

    def deal(pieces):
        return pieces[:1] + [over_tp(pieces[k], k) for k in range(1, tp)]

    def pick(weights, k):
        return lax.dynamic_index_in_dim(weights, me ^ k, 0, keepdims=False)

    pairs = deal(
        [jnp.concatenate([pick(expert_gate, k), pick(expert_up, k)], axis=1) for k in range(tp)]
    )
    downs = deal([pick(expert_down, k) for k in range(tp)])

    spread, pick0, pick1 = call(
        functools.partial(route_kernel, experts, cap),
        [
            jax.ShapeDtypeStruct((experts * cap, tok), BF16),
            jax.ShapeDtypeStruct((tok, experts * cap), BF16),
            jax.ShapeDtypeStruct((tok, experts * cap), BF16),
        ],
        (routes.T,),
    )
    gain = norm_gain.astype(F32).reshape(tp, 1, width)

    mixed = call(
        functools.partial(attn_kernel, nz, tok),
        [jax.ShapeDtypeStruct((half, 128), BF16)] * nz,
        (core_ref, z_ref, *owns, *swapped),
        smem=2,
        scratch=(
            pltpu.VMEM((nz, 2 * tok, 128), BF16),
            pltpu.VMEM((nz, 2 * tok, 128), BF16),
            pltpu.VMEM((nz, 8, 2 * tok), F32),
            pltpu.VMEM((nz, half, 128), BF16),
            pltpu.VMEM((nz, half, 128), BF16),
        ),
    )
    back = [mixed[0]] + [over_z(mixed[k], k) for k in range(1, nz)]
    attended = jnp.stack(back)
    attended_all = all_tp(attended)
    mid, outgoing = call(
        functools.partial(mid_kernel, heads, cap),
        [
            jax.ShapeDtypeStruct((tok, width), BF16),
            jax.ShapeDtypeStruct((experts, cap, width), BF16),
        ],
        (me_ref, z_ref, *attended_all, out_weight, residual, spread),
        smem=2,
    )
    arrived = lax.all_to_all(outgoing, ("sp", "tp"), 0, 0, tiled=True)
    mids = all_tp(mid)
    produced = call(
        functools.partial(expert_kernel, sp, tp),
        jax.ShapeDtypeStruct((sp * tp, cap, width), BF16),
        (me_ref, arrived, gain, *pairs, *downs),
        smem=1,
        scratch=(
            pltpu.VMEM((sp * cap, tp * width), BF16),
            pltpu.VMEM((sp * cap, tp * expert_gate.shape[2]), BF16),
        ),
    )
    returned = lax.all_to_all(produced, ("sp", "tp"), 0, 0, tiled=True)
    shared_mid = call(
        shared_kernel,
        jax.ShapeDtypeStruct((tok, shared_gate.shape[1]), BF16),
        (me_ref, *mids, gain, shared_gate, shared_up),
        smem=1,
    )
    shared_mids = all_tp(shared_mid)
    return call(
        final_kernel,
        jax.ShapeDtypeStruct((tok, width), BF16),
        (me_ref, *shared_mids, shared_down, mid, returned, pick0, pick1, route_weight.T),
        smem=1,
        scratch=(pltpu.VMEM((tok, shared_down.shape[0]), BF16),),
    )


def slot_targets(routes, experts_all, capacity):
    flat_routes = routes.reshape(-1)
    onehot = (flat_routes[:, None] == jnp.arange(experts_all, dtype=jnp.int32)[None, :]).astype(
        jnp.int32
    )
    before = jnp.cumsum(onehot, axis=0) - onehot
    return flat_routes * capacity + jnp.sum(before * onehot, axis=1)


def keep_state(fold_state):
    return fold_state


def generic_shards(
    queries,
    key_vectors,
    value_vectors,
    log_gate_sums,
    residual,
    out_weight,
    norm_gain,
    routes,
    route_weight,
    expert_gate,
    expert_up,
    expert_down,
    shared_gate,
    shared_up,
    shared_down,
):
    tok_dev = queries.shape[0]
    head_dim = HDIM
    local_heads = log_gate_sums.shape[1]
    local_width = residual.shape[1]
    model_width = norm_gain.shape[0]
    score_scale = head_dim ** (-0.5)
    seq_first = lax.axis_index("sp") * tok_dev
    query_heads = queries.reshape(tok_dev, local_heads, head_dim)
    query_pos = seq_first + jnp.arange(tok_dev, dtype=jnp.int32)
    own_gates = log_gate_sums.T
    all_gates = lax.all_gather(log_gate_sums, "sp", axis=0, tiled=True)
    initial = (
        jnp.full((local_heads, tok_dev), -1e30, jnp.float32),
        jnp.zeros((local_heads, tok_dev), jnp.float32),
        jnp.zeros((local_heads, tok_dev, head_dim), jnp.float32),
    )
    key_heads = key_vectors.reshape(tok_dev, local_heads, head_dim)
    value_heads = value_vectors.reshape(tok_dev, local_heads, head_dim)
    key_part = lax.all_gather(key_heads, "sp", axis=0, tiled=True)
    value_part = lax.all_gather(value_heads, "sp", axis=0, tiled=True)
    part_rows = key_part.shape[0]
    block_size = math.gcd(part_rows, 512)
    key_blocks = key_part.reshape(part_rows // block_size, block_size, local_heads, head_dim)
    value_blocks = value_part.reshape(part_rows // block_size, block_size, local_heads, head_dim)

    def one_block(fold_state, inputs):
        key_block, value_block, block_number = inputs
        block_first = block_number * block_size

        def compute(old_state):
            running_max, weight_total, summed = old_state
            gate_block = lax.dynamic_slice_in_dim(all_gates, block_first, block_size, 0).T
            scores = (
                jnp.einsum(
                    "qhd,khd->hqk", query_heads, key_block, preferred_element_type=jnp.float32
                )
                * score_scale
            )
            scores = scores + own_gates[:, :, None] - gate_block[:, None, :]
            key_pos = block_first + jnp.arange(block_size, dtype=jnp.int32)
            allowed = (key_pos[None, :] <= query_pos[:, None])[None]
            newmax = jnp.maximum(running_max, jnp.max(jnp.where(allowed, scores, -jnp.inf), axis=2))
            factor = jnp.exp(running_max - newmax)
            weight = jnp.where(allowed, jnp.exp(scores - newmax[:, :, None]), 0.0)
            weight_total = weight_total * factor + jnp.sum(weight, axis=2)
            summed = summed * factor[:, :, None] + jnp.einsum(
                "hqk,khd->hqd",
                weight.astype(jnp.bfloat16),
                value_block,
                preferred_element_type=jnp.float32,
            )
            return (newmax, weight_total, summed)

        useful = block_first <= seq_first + tok_dev - 1
        return (lax.cond(useful, compute, keep_state, fold_state), None)

    numbers = jnp.arange(part_rows // block_size, dtype=jnp.int32)
    result_state, _ = lax.scan(one_block, initial, (key_blocks, value_blocks, numbers))
    _, weight_total, summed = result_state
    attended = (summed / weight_total[:, :, None]).astype(jnp.bfloat16)
    attended = attended.transpose(1, 0, 2).reshape(tok_dev, local_heads * head_dim)
    weight_rows = out_weight
    projected = jnp.dot(
        lax.all_gather(attended, "tp", axis=1, tiled=True),
        weight_rows,
        preferred_element_type=jnp.float32,
    )
    mid = (residual.astype(jnp.float32) + projected).astype(jnp.bfloat16)
    mid_wide = mid.astype(jnp.float32)
    feature_first = lax.axis_index("tp") * local_width
    squares = lax.psum(jnp.sum(mid_wide * mid_wide, axis=1), "tp")
    inverse = lax.rsqrt(squares / model_width + EPSILON)
    own_gain = lax.dynamic_slice_in_dim(norm_gain, feature_first, local_width, 0).astype(
        jnp.float32
    )
    normed_own = (mid_wide * inverse[:, None] * own_gain[None, :]).astype(jnp.bfloat16)
    normed = lax.all_gather(normed_own, "tp", axis=1, tiled=True)
    shared_mid = silu_gate(
        jnp.dot(normed, shared_gate, preferred_element_type=jnp.float32),
        jnp.dot(normed, shared_up, preferred_element_type=jnp.float32),
    ).astype(jnp.bfloat16)
    weight_rows = shared_down
    shared_out = jnp.dot(
        lax.all_gather(shared_mid, "tp", axis=1, tiled=True),
        weight_rows,
        preferred_element_type=jnp.float32,
    )
    exp_dev = expert_gate.shape[0]
    sp_count = lax.axis_size("sp")
    experts_all = exp_dev * sp_count
    top_count = routes.shape[1]
    capacity = 5 * tok_dev * top_count // (4 * experts_all)
    targets = slot_targets(routes, experts_all, capacity)
    owners = (
        jnp.full((experts_all * capacity,), tok_dev, jnp.int32)
        .at[targets]
        .set(jnp.arange(tok_dev * top_count, dtype=jnp.int32) // top_count)
    )
    padded = jnp.concatenate(
        [normed_own, jnp.zeros((1, normed_own.shape[1]), jnp.bfloat16)], axis=0
    )
    outgoing = padded[owners].reshape(sp_count, exp_dev, capacity, normed_own.shape[1])
    rows_all = lax.all_gather(
        lax.all_to_all(outgoing, "sp", split_axis=0, concat_axis=0, tiled=True),
        "tp",
        axis=3,
        tiled=True,
    )
    gate_part = jnp.einsum(
        "secd,edf->secf", rows_all, expert_gate, preferred_element_type=jnp.float32
    )
    up_part = jnp.einsum("secd,edf->secf", rows_all, expert_up, preferred_element_type=jnp.float32)
    hidden = silu_gate(gate_part, up_part).astype(jnp.bfloat16)
    hidden_all = lax.all_gather(hidden, "tp", axis=3, tiled=True)
    produced = jnp.einsum(
        "secf,efd->secd", hidden_all, expert_down, preferred_element_type=jnp.float32
    ).astype(jnp.bfloat16)
    returned = lax.all_to_all(produced, "sp", split_axis=0, concat_axis=0, tiled=True)
    returned_flat = returned.reshape(experts_all * capacity, local_width)
    picked = returned_flat[targets].astype(jnp.float32).reshape(tok_dev, top_count, local_width)
    routed = jnp.sum(picked * route_weight[:, :, None], axis=1)
    return (mid_wide + shared_out + routed).astype(jnp.bfloat16)


def layer(*args):
    return shards(*args)


def solution(mesh):
    placed = (
        P("sp", "tp"),
        P("sp", "tp"),
        P("sp", "tp"),
        P("sp", "tp"),
        P("sp", "tp"),
        P(None, "tp"),
        P(),
        P("sp", None),
        P("sp", None),
        P("sp", None, "tp"),
        P("sp", None, "tp"),
        P("sp", None, "tp"),
        P(None, "tp"),
        P(None, "tp"),
        P(None, "tp"),
    )
    sp, tp = mesh.shape["sp"], mesh.shape["tp"]

    def program(*args):
        heads = args[3].shape[1] // tp
        exp_dev = args[9].shape[0] // sp
        deals = sp % 2 == 0 and heads * 2 == sp and exp_dev == tp and tp & (tp - 1) == 0
        body = layer if deals else generic_shards
        mapped = jax.shard_map(body, mesh=mesh, in_specs=placed, out_specs=P("sp", "tp"), check_vma=False)
        return mapped(*args)

    return program
```

profile of v0, /device:TPU:0, one launch (start us, length us, event | category | flops | bytes accessed | tf_op | source)
XLA Modules:
  0.0 235.4 jit_solution(14671505582187095688)
XLA Ops:
  0.0 2.3 shard_map.145
  2.4 3.1 %collective-permute-start = (bf16[784,128]{1,0:T(8,128)(2,1)}, bf16[784,128]{1,0:T(8,128)(2,1)S(1)}, u32[]{:S(2)}, u32[]{:S(2)}) collective-permute-start(bf16[784,128]{1,0:T(8,128)(2,1)} %get-tuple-element.19), channel_id=1, source_target_pairs={{0,8},{4,12},{8,0},{12,4},{16,24},{20,28},{24,16},{28,20},{1,9},{5... | collective-permute-start | bytes 602120 | tf_op jit(solution)/shard_map/ppermute | solution.py:298
  5.4 2.6 %collective-permute-start.1 = (bf16[784,128]{1,0:T(8,128)(2,1)}, bf16[784,128]{1,0:T(8,128)(2,1)S(1)}, u32[]{:S(2)}, u32[]{:S(2)}) collective-permute-start(bf16[784,128]{1,0:T(8,128)(2,1)} %get-tuple-element.20), channel_id=1, source_target_pairs={{0,16},{4,20},{8,24},{12,28},{16,0},{20,4},{24,8},{28,12},{1,17},{... | collective-permute-start | bytes 602120 | tf_op jit(solution)/shard_map/ppermute | solution.py:298
  8.0 6.2 %collective-permute-done.refs_1_ = bf16[784,128]{1,0:T(8,128)(2,1)S(1)} collective-permute-done((bf16[784,128]{1,0:T(8,128)(2,1)}, bf16[784,128]{1,0:T(8,128)(2,1)S(1)}, u32[]{:S(2)}, u32[]{:S(2)}) %collective-permute-start) | collective-permute-done | bytes 200736 | tf_op jit(solution)/shard_map/ppermute | solution.py:298
  14.2 8.8 %collective-permute-done.1.refs_2_ = bf16[784,128]{1,0:T(8,128)(2,1)S(1)} collective-permute-done((bf16[784,128]{1,0:T(8,128)(2,1)}, bf16[784,128]{1,0:T(8,128)(2,1)S(1)}, u32[]{:S(2)}, u32[]{:S(2)}) %collective-permute-start.1) | collective-permute-done | bytes 200736 | tf_op jit(solution)/shard_map/ppermute | solution.py:298
  23.5 0.9 collective-permute-done.5.refs_6_
  25.4 14.9 %shard_map.146 = (bf16[256,128]{1,0:T(8,128)(2,1)}, bf16[256,128]{1,0:T(8,128)(2,1)}, bf16[256,128]{1,0:T(8,128)(2,1)}, bf16[256,128]{1,0:T(8,128)(2,1)}) custom-call(s32[1]{0:T(128)} %bitcast.2.c_ref, s32[1]{0:T(128)} %bitcast.1.z_ref, bf16[784,128]{1,0:T(8,128)(2,1)} %get-tuple-element.18.refs_0_, bf16[784,128]{1,0:T(8,128)(2,1)} %copy-done.17, ...), custom_call_target="tpu_custom_call" | custom-call | tf_op jit(solution)/shard_map/pallas_call | solution.py:28
  40.3 3.2 %collective-permute-start.7 = (bf16[256,128]{1,0:T(8,128)(2,1)}, bf16[256,128]{1,0:T(8,128)(2,1)S(1)}, u32[]{:S(2)}, u32[]{:S(2)}) collective-permute-start(bf16[256,128]{1,0:T(8,128)(2,1)} %get-tuple-element.23), channel_id=1, source_target_pairs={{0,8},{4,12},{8,0},{12,4},{16,24},{20,28},{24,16},{28,20},{1,9},{5... | collective-permute-start | bytes 196616 | tf_op jit(solution)/shard_map/ppermute | solution.py:298
  43.5 1.1 collective-permute-start.8
  44.6 1.4 collective-permute-start.9
  46.1 5.8 %collective-permute-done.8 = bf16[256,128]{1,0:T(8,128)(2,1)S(1)} collective-permute-done((bf16[256,128]{1,0:T(8,128)(2,1)}, bf16[256,128]{1,0:T(8,128)(2,1)S(1)}, u32[]{:S(2)}, u32[]{:S(2)}) %collective-permute-start.8) | collective-permute-done | bytes 65568 | tf_op jit(solution)/shard_map/ppermute | solution.py:298
  52.0 0.9 pad_maximum_fusion.4.refs_0_
  52.9 1.6 collective-permute-start.10
  54.4 1.5 collective-permute-start.11
  56.4 3.9 %shard_map.147 = (bf16[1280,512]{1,0:T(8,128)(2,1)}, bf16[512,1280]{1,0:T(8,128)(2,1)}, bf16[512,1280]{1,0:T(8,128)(2,1)}) custom-call(s32[2,512]{1,0:T(2,128)} %bitcast.42), custom_call_target="tpu_custom_call" | custom-call | tf_op jit(solution)/shard_map/pallas_call | solution.py:28
  60.3 1.8 collective-permute-done.10.refs_1_
  62.1 4.5 %collective-permute-done.11.refs_2_ = bf16[4,256,128]{2,1,0:T(8,128)(2,1)S(1)} collective-permute-done((bf16[4,256,128]{2,1,0:T(8,128)(2,1)S(1)}, bf16[4,256,128]{2,1,0:T(8,128)(2,1)S(1)}, u32[]{:S(2)}, u32[]{:S(2)}) %collective-permute-start.11) | collective-permute-done | bytes 262176 | tf_op jit(solution)/shard_map/ppermute | solution.py:289
  66.6 0.7 copy-done.15
  67.4 4.8 %shard_map.148 = (bf16[512,512]{1,0:T(8,128)(2,1)}, bf16[32,40,512]{2,1,0:T(8,128)(2,1)}) custom-call(s32[1]{0:T(128)} %bitcast.t_ref, s32[1]{0:T(128)} %bitcast.1.z_ref, bf16[4,256,128]{2,1,0:T(8,128)(2,1)} %copy-done.5, bf16[4,256,128]{2,1,0:T(8,128)(2,1)} %copy-done.14, bf16[4,256,128]{2,1,0:T(8,128)(2,1)} %copy-done.15, bf16[4,256,128]{2,1,0:T(8,128)(2,1)} %copy-done.16, ...), custom_call_target="tpu_custom_call" | custom-call | tf_op jit(solution)/shard_map/pallas_call | solution.py:28
  72.1 4.6 %all-to-all-start = ((bf16[32,40,512]{2,1,0:T(8,128)(2,1)}), bf16[32,40,512]{2,1,0:T(8,128)(2,1)S(1)}, u32[]{:S(2)}, u32[]{:S(2)}) async-start(bf16[32,40,512]{2,1,0:T(8,128)(2,1)} %get-tuple-element.28), calls=%async_computation | async-start | bytes 2621440 | tf_op jit(solution)/shard_map/all_to_all | solution.py:357
  76.7 1.8 dynamic-slice_bitcast_fusion.4
  78.7 1.8 collective-permute-start.19
  80.6 1.5 collective-permute-start.20
  82.1 0.9 dynamic-slice_bitcast_fusion
  83.1 0.6 collective-permute-start.22
  83.8 1.5 collective-permute-start.21
  85.3 1.5 collective-permute-start.23
  86.8 41.1 %collective-permute-done.22.refs_5_ = bf16[512,512]{1,0:T(8,128)(2,1)S(1)} collective-permute-done((bf16[512,512]{1,0:T(8,128)(2,1)S(1)}, bf16[512,512]{1,0:T(8,128)(2,1)S(1)}, u32[]{:S(2)}, u32[]{:S(2)}) %collective-permute-start.22) | collective-permute-done | bytes 524320 | tf_op jit(solution)/shard_map/ppermute | solution.py:289
  127.9 1.6 collective-permute-start.24
  129.5 0.6 reshape.19
  130.1 1.1 pad_maximum_fusion.refs_0_
  131.2 30.7 %collective-permute-done.24.refs_7_ = bf16[512,512]{1,0:T(8,128)(2,1)S(1)} collective-permute-done((bf16[512,512]{1,0:T(8,128)(2,1)S(1)}, bf16[512,512]{1,0:T(8,128)(2,1)S(1)}, u32[]{:S(2)}, u32[]{:S(2)}) %collective-permute-start.24) | collective-permute-done | bytes 524320 | tf_op jit(solution)/shard_map/ppermute | solution.py:289
  161.9 0.8 copy-done.13
  163.1 0.6 copy-done.7
  164.1 6.8 %shard_map.150 = bf16[32,40,512]{2,1,0:T(8,128)(2,1)} custom-call(s32[1]{0:T(128)} %bitcast.t_ref, bf16[32,40,512]{2,1,0:T(8,128)(2,1)} %copy-done.1, f32[4,1,512]{2,1,0:T(1,128)} %bitcast.35, bf16[2048,256]{1,0:T(8,128)(2,1)} %pad_maximum_fusion.refs_0_, bf16[2048,256]{1,0:T(8,128)(2,1)} %copy-done.6, bf16[2048,256]{1,0:T(8,128)(2,1)} %copy-done.7, ...), custom_call_target="tpu_custom_call" | custom-call | tf_op jit(solution)/shard_map/pallas_call | solution.py:28
  171.0 4.7 %all-to-all-start.1 = ((bf16[32,40,512]{2,1,0:T(8,128)(2,1)}), bf16[32,40,512]{2,1,0:T(8,128)(2,1)S(1)}, u32[]{:S(2)}, u32[]{:S(2)}) async-start(bf16[32,40,512]{2,1,0:T(8,128)(2,1)} %shard_map.150), calls=%async_computation.1 | async-start | bytes 2621440 | tf_op jit(solution)/shard_map/all_to_all | solution.py:369
  175.7 1.7 collective-permute-start.13
  177.3 1.5 collective-permute-start.14
  179.2 23.9 %collective-permute-done.13.refs_1_ = bf16[512,512]{1,0:T(8,128)(2,1)S(1)} collective-permute-done((bf16[512,512]{1,0:T(8,128)(2,1)S(1)}, bf16[512,512]{1,0:T(8,128)(2,1)S(1)}, u32[]{:S(2)}, u32[]{:S(2)}) %collective-permute-start.13) | collective-permute-done | bytes 524320 | tf_op jit(solution)/shard_map/ppermute | solution.py:289
  203.1 13.0 %collective-permute-done.15.refs_3_ = bf16[512,512]{1,0:T(8,128)(2,1)S(1)} collective-permute-done((bf16[512,512]{1,0:T(8,128)(2,1)S(1)}, bf16[512,512]{1,0:T(8,128)(2,1)S(1)}, u32[]{:S(2)}, u32[]{:S(2)}) %collective-permute-start.15) | collective-permute-done | bytes 524320 | tf_op jit(solution)/shard_map/ppermute | solution.py:289
  216.2 0.8 copy-done.10
  217.0 3.7 %shard_map.149.refs_0_ = bf16[512,128]{1,0:T(8,128)(2,1)} custom-call(s32[1]{0:T(128)} %bitcast.t_ref, bf16[512,512]{1,0:T(8,128)(2,1)} %get-tuple-element.27.refs_0_.refs_5_, bf16[512,512]{1,0:T(8,128)(2,1)} %copy-done.8, bf16[512,512]{1,0:T(8,128)(2,1)} %copy-done.9, bf16[512,512]{1,0:T(8,128)(2,1)} %copy-done.10, f32[4,1,512]{2,1,0:T(1,128)} %bitcast.36, ...), custom_call_target="tpu_custom_call" | custom-call | tf_op jit(solution)/shard_map/pallas_call | solution.py:28
  220.7 0.5 collective-permute-start.16
  221.5 2.6 %collective-permute-start.18 = (bf16[512,128]{1,0:T(8,128)(2,1)}, bf16[512,128]{1,0:T(8,128)(2,1)S(1)}, u32[]{:S(2)}, u32[]{:S(2)}) collective-permute-start(bf16[512,128]{1,0:T(8,128)(2,1)} %shard_map.149.refs_0_), channel_id=1, source_target_pairs={{0,3},{1,2},{2,1},{3,0},{4,7},{5,6},{6,5},{7,4},{8,11},{9,10},{10,... | collective-permute-start | bytes 393224 | tf_op jit(solution)/shard_map/ppermute | solution.py:289
  224.2 3.1 %collective-permute-done.16.refs_1_ = bf16[512,128]{1,0:T(8,128)(2,1)S(1)} collective-permute-done((bf16[512,128]{1,0:T(8,128)(2,1)}, bf16[512,128]{1,0:T(8,128)(2,1)S(1)}, u32[]{:S(2)}, u32[]{:S(2)}) %collective-permute-start.16) | collective-permute-done | bytes 131104 | tf_op jit(solution)/shard_map/ppermute | solution.py:289
  227.2 1.6 collective-permute-done.17.refs_2_
  228.9 0.6 copy-done.25
  230.0 5.4 %shard_map.151 = bf16[512,512]{1,0:T(8,128)(2,1)} custom-call(s32[1]{0:T(128)} %bitcast.t_ref, bf16[512,128]{1,0:T(8,128)(2,1)} %shard_map.149.refs_0_, bf16[512,128]{1,0:T(8,128)(2,1)} %copy-done.24, bf16[512,128]{1,0:T(8,128)(2,1)} %copy-done.25, bf16[512,128]{1,0:T(8,128)(2,1)} %copy-done.26, bf16[512,512]{1,0:T(8,128)(2,1)} %refs_4_.3, ...), custom_call_target="tpu_custom_call" | custom-call | tf_op jit(solution)/shard_map/pallas_call | solution.py:28
  (77 shorter events, 4.7 us)
Async XLA Ops:
  2.4 11.8 %collective-permute-start = (bf16[784,128]{1,0:T(8,128)(2,1)}, bf16[784,128]{1,0:T(8,128)(2,1)S(1)}, u32[]{:S(2)}, u32[]{:S(2)}) collective-permute-start(bf16[784,128]{1,0:T(8,128)(2,1)} %get-tuple-element.19), channel_id=1, source_target_pairs={{0,8},{4,12},{8,0},{12,4},{16,24},{20,28},{24,16},{28,20},{1,9},{5... | collective-permute-start | bytes 602120 | tf_op jit(solution)/shard_map/ppermute | solution.py:298
  5.4 17.6 %collective-permute-start.1 = (bf16[784,128]{1,0:T(8,128)(2,1)}, bf16[784,128]{1,0:T(8,128)(2,1)S(1)}, u32[]{:S(2)}, u32[]{:S(2)}) collective-permute-start(bf16[784,128]{1,0:T(8,128)(2,1)} %get-tuple-element.20), channel_id=1, source_target_pairs={{0,16},{4,20},{8,24},{12,28},{16,0},{20,4},{24,8},{28,12},{1,17},{... | collective-permute-start | bytes 602120 | tf_op jit(solution)/shard_map/ppermute | solution.py:298
  8.0 15.0 %collective-permute-start.2 = (bf16[784,128]{1,0:T(8,128)(2,1)}, bf16[784,128]{1,0:T(8,128)(2,1)S(1)}, u32[]{:S(2)}, u32[]{:S(2)}) collective-permute-start(bf16[784,128]{1,0:T(8,128)(2,1)} %get-tuple-element.21), channel_id=1, source_target_pairs={{0,24},{4,28},{8,16},{12,20},{16,8},{20,12},{24,0},{28,4},{1,25},{... | collective-permute-start | bytes 602120 | tf_op jit(solution)/shard_map/ppermute | solution.py:298
  8.0 15.5 %collective-permute-start.3 = (bf16[784,128]{1,0:T(8,128)(2,1)}, bf16[784,128]{1,0:T(8,128)(2,1)S(1)}, u32[]{:S(2)}, u32[]{:S(2)}) collective-permute-start(bf16[784,128]{1,0:T(8,128)(2,1)} %get-tuple-element.18.refs_0_), channel_id=1, source_target_pairs={{0,4},{4,0},{8,12},{12,8},{16,20},{20,16},{24,28},{28,24},{1,5},{5... | collective-permute-start | bytes 602120 | tf_op jit(solution)/shard_map/ppermute | solution.py:308
  14.2 10.6 %copy-start.17 = (bf16[784,128]{1,0:T(8,128)(2,1)}, bf16[784,128]{1,0:T(8,128)(2,1)S(1)}, u32[]{:S(2)}) copy-start(bf16[784,128]{1,0:T(8,128)(2,1)S(1)} %collective-permute-done.refs_1_) | copy-start | bytes 602116
  14.2 9.3 %collective-permute-start.4 = (bf16[784,128]{1,0:T(8,128)(2,1)S(1)}, bf16[784,128]{1,0:T(8,128)(2,1)S(1)}, u32[]{:S(2)}, u32[]{:S(2)}) collective-permute-start(bf16[784,128]{1,0:T(8,128)(2,1)S(1)} %collective-permute-done.refs_1_), channel_id=1, source_target_pairs={{0,4},{4,0},{8,12},{12,8},{16,20},{20,16},{24,28},{28,24},{1,5},{5... | collective-permute-start | bytes 602120 | tf_op jit(solution)/shard_map/ppermute | solution.py:308
  23.0 1.7 copy-start.18
  23.0 1.4 collective-permute-start.5
  23.0 1.7 copy-start.19
  23.0 1.7 collective-permute-start.6
  23.5 1.2 copy-start.20
  23.5 1.2 copy-start.21
  40.3 5.8 %collective-permute-start.7 = (bf16[256,128]{1,0:T(8,128)(2,1)}, bf16[256,128]{1,0:T(8,128)(2,1)S(1)}, u32[]{:S(2)}, u32[]{:S(2)}) collective-permute-start(bf16[256,128]{1,0:T(8,128)(2,1)} %get-tuple-element.23), channel_id=1, source_target_pairs={{0,8},{4,12},{8,0},{12,4},{16,24},{20,28},{24,16},{28,20},{1,9},{5... | collective-permute-start | bytes 196616 | tf_op jit(solution)/shard_map/ppermute | solution.py:298
  43.5 8.4 %collective-permute-start.8 = (bf16[256,128]{1,0:T(8,128)(2,1)}, bf16[256,128]{1,0:T(8,128)(2,1)S(1)}, u32[]{:S(2)}, u32[]{:S(2)}) collective-permute-start(bf16[256,128]{1,0:T(8,128)(2,1)} %get-tuple-element.24), channel_id=1, source_target_pairs={{0,16},{4,20},{8,24},{12,28},{16,0},{20,4},{24,8},{28,12},{1,17},{... | collective-permute-start | bytes 196616 | tf_op jit(solution)/shard_map/ppermute | solution.py:298
  44.6 7.4 %collective-permute-start.9 = (bf16[256,128]{1,0:T(8,128)(2,1)}, bf16[256,128]{1,0:T(8,128)(2,1)S(1)}, u32[]{:S(2)}, u32[]{:S(2)}) collective-permute-start(bf16[256,128]{1,0:T(8,128)(2,1)} %get-tuple-element.25), channel_id=1, source_target_pairs={{0,24},{4,28},{8,16},{12,20},{16,8},{20,12},{24,0},{28,4},{1,25},{... | collective-permute-start | bytes 196616 | tf_op jit(solution)/shard_map/ppermute | solution.py:298
  52.8 13.7 %copy-start.5 = (bf16[4,256,128]{2,1,0:T(8,128)(2,1)}, bf16[4,256,128]{2,1,0:T(8,128)(2,1)S(1)}, u32[]{:S(2)}) copy-start(bf16[4,256,128]{2,1,0:T(8,128)(2,1)S(1)} %pad_maximum_fusion.4.refs_0_) | copy-start | bytes 786436
  52.9 9.2 %collective-permute-start.10 = (bf16[4,256,128]{2,1,0:T(8,128)(2,1)S(1)}, bf16[4,256,128]{2,1,0:T(8,128)(2,1)S(1)}, u32[]{:S(2)}, u32[]{:S(2)}) collective-permute-start(bf16[4,256,128]{2,1,0:T(8,128)(2,1)S(1)} %pad_maximum_fusion.4.refs_0_), channel_id=1, source_target_pairs={{0,1},{1,0},{2,3},{3,2},{4,5},{5,4},{6,7},{7,6},{8,9},{9,8},{10,11... | collective-permute-start | bytes 786440 | tf_op jit(solution)/shard_map/ppermute | solution.py:289
  54.4 12.1 %collective-permute-start.11 = (bf16[4,256,128]{2,1,0:T(8,128)(2,1)S(1)}, bf16[4,256,128]{2,1,0:T(8,128)(2,1)S(1)}, u32[]{:S(2)}, u32[]{:S(2)}) collective-permute-start(bf16[4,256,128]{2,1,0:T(8,128)(2,1)S(1)} %pad_maximum_fusion.4.refs_0_), channel_id=1, source_target_pairs={{0,2},{1,3},{2,0},{3,1},{4,6},{5,7},{6,4},{7,5},{8,10},{9,11},{10,... | collective-permute-start | bytes 786440 | tf_op jit(solution)/shard_map/ppermute | solution.py:289
  55.9 10.6 %collective-permute-start.12 = (bf16[4,256,128]{2,1,0:T(8,128)(2,1)S(1)}, bf16[4,256,128]{2,1,0:T(8,128)(2,1)S(1)}, u32[]{:S(2)}, u32[]{:S(2)}) collective-permute-start(bf16[4,256,128]{2,1,0:T(8,128)(2,1)S(1)} %pad_maximum_fusion.4.refs_0_), channel_id=1, source_target_pairs={{0,3},{1,2},{2,1},{3,0},{4,7},{5,6},{6,5},{7,4},{8,11},{9,10},{10,... | collective-permute-start | bytes 786440 | tf_op jit(solution)/shard_map/ppermute | solution.py:289
  62.1 4.5 %copy-start.14 = (bf16[4,256,128]{2,1,0:T(8,128)(2,1)}, bf16[4,256,128]{2,1,0:T(8,128)(2,1)S(1)}, u32[]{:S(2)}) copy-start(bf16[4,256,128]{2,1,0:T(8,128)(2,1)S(1)} %collective-permute-done.10.refs_1_) | copy-start | bytes 786436
  72.1 4.6 %copy-start.2 = (bf16[4,2048,128]{2,1,0:T(8,128)(2,1)S(1)}, bf16[4,2048,128]{2,1,0:T(8,128)(2,1)}, u32[]{:S(2)}) copy-start(bf16[4,2048,128]{2,1,0:T(8,128)(2,1)} %param.25) | copy-start | bytes 6291460
  72.1 90.6 %all-to-all-start = ((bf16[32,40,512]{2,1,0:T(8,128)(2,1)}), bf16[32,40,512]{2,1,0:T(8,128)(2,1)S(1)}, u32[]{:S(2)}, u32[]{:S(2)}) async-start(bf16[32,40,512]{2,1,0:T(8,128)(2,1)} %get-tuple-element.28), calls=%async_computation | async-start | bytes 2621440 | tf_op jit(solution)/shard_map/all_to_all | solution.py:357
  78.5 3.6 %copy-start.3 = (bf16[4,512,512]{2,1,0:T(8,128)(2,1)S(1)}, bf16[4,512,512]{2,1,0:T(8,128)(2,1)}, u32[]{:S(2)}) copy-start(bf16[4,512,512]{2,1,0:T(8,128)(2,1)} %param.26) | copy-start | bytes 6291460
  78.7 83.2 %collective-permute-start.19 = (bf16[2048,256]{1,0:T(8,128)(2,1)S(1)}, bf16[2048,256]{1,0:T(8,128)(2,1)S(1)}, u32[]{:S(2)}, u32[]{:S(2)}) collective-permute-start(bf16[2048,256]{1,0:T(8,128)(2,1)S(1)} %pad_maximum_fusion.1), channel_id=1, source_target_pairs={{0,1},{1,0},{2,3},{3,2},{4,5},{5,4},{6,7},{7,6},{8,9},{9,8},{10,11... | collective-permute-start | bytes 3145736 | tf_op jit(solution)/shard_map/ppermute | solution.py:289
  80.6 81.3 %collective-permute-start.20 = (bf16[2048,256]{1,0:T(8,128)(2,1)S(1)}, bf16[2048,256]{1,0:T(8,128)(2,1)S(1)}, u32[]{:S(2)}, u32[]{:S(2)}) collective-permute-start(bf16[2048,256]{1,0:T(8,128)(2,1)S(1)} %pad_maximum_fusion.2), channel_id=1, source_target_pairs={{0,2},{1,3},{2,0},{3,1},{4,6},{5,7},{6,4},{7,5},{8,10},{9,11},{10,... | collective-permute-start | bytes 3145736 | tf_op jit(solution)/shard_map/ppermute | solution.py:289
  83.1 46.4 %copy-start.27 = (bf16[2048]{0:T(1024)(128)(2,1)S(1)}, bf16[2048]{0:T(1024)(128)(2,1)}, u32[]{:S(2)}) copy-start(bf16[2048]{0:T(1024)(128)(2,1)} %param.21) | copy-start | bytes 12292
  83.1 44.8 %collective-permute-start.22 = (bf16[512,512]{1,0:T(8,128)(2,1)S(1)}, bf16[512,512]{1,0:T(8,128)(2,1)S(1)}, u32[]{:S(2)}, u32[]{:S(2)}) collective-permute-start(bf16[512,512]{1,0:T(8,128)(2,1)S(1)} %get-tuple-element.32), channel_id=1, source_target_pairs={{0,1},{1,0},{2,3},{3,2},{4,5},{5,4},{6,7},{7,6},{8,9},{9,8},{10,11... | collective-permute-start | bytes 1572872 | tf_op jit(solution)/shard_map/ppermute | solution.py:289
  83.8 78.9 %collective-permute-start.21 = (bf16[2048,256]{1,0:T(8,128)(2,1)S(1)}, bf16[2048,256]{1,0:T(8,128)(2,1)}, u32[]{:S(2)}, u32[]{:S(2)}) collective-permute-start(bf16[2048,256]{1,0:T(8,128)(2,1)S(1)} %pad_maximum_fusion.3), channel_id=1, source_target_pairs={{0,3},{1,2},{2,1},{3,0},{4,7},{5,6},{6,5},{7,4},{8,11},{9,10},{10,... | collective-permute-start | bytes 3145736 | tf_op jit(solution)/shard_map/ppermute | solution.py:289
  85.3 45.9 %collective-permute-start.23 = (bf16[512,512]{1,0:T(8,128)(2,1)S(1)}, bf16[512,512]{1,0:T(8,128)(2,1)S(1)}, u32[]{:S(2)}, u32[]{:S(2)}) collective-permute-start(bf16[512,512]{1,0:T(8,128)(2,1)S(1)} %get-tuple-element.34), channel_id=1, source_target_pairs={{0,2},{1,3},{2,0},{3,1},{4,6},{5,7},{6,4},{7,5},{8,10},{9,11},{10,... | collective-permute-start | bytes 1572872 | tf_op jit(solution)/shard_map/ppermute | solution.py:289
  127.9 34.0 %copy-start.11 = (bf16[512,512]{1,0:T(8,128)(2,1)}, bf16[512,512]{1,0:T(8,128)(2,1)S(1)}, u32[]{:S(2)}) copy-start(bf16[512,512]{1,0:T(8,128)(2,1)S(1)} %collective-permute-done.22.refs_5_) | copy-start | bytes 1572868
  127.9 34.0 %collective-permute-start.24 = (bf16[512,512]{1,0:T(8,128)(2,1)S(1)}, bf16[512,512]{1,0:T(8,128)(2,1)S(1)}, u32[]{:S(2)}, u32[]{:S(2)}) collective-permute-start(bf16[512,512]{1,0:T(8,128)(2,1)S(1)} %get-tuple-element.31), channel_id=1, source_target_pairs={{0,3},{1,2},{2,1},{3,0},{4,7},{5,6},{6,5},{7,4},{8,11},{9,10},{10,... | collective-permute-start | bytes 1572872 | tf_op jit(solution)/shard_map/ppermute | solution.py:289
  131.2 30.7 %copy-start.12 = (bf16[512,512]{1,0:T(8,128)(2,1)}, bf16[512,512]{1,0:T(8,128)(2,1)S(1)}, u32[]{:S(2)}) copy-start(bf16[512,512]{1,0:T(8,128)(2,1)S(1)} %collective-permute-done.23.refs_6_) | copy-start | bytes 1572868
  161.9 1.2 copy-start.6
  162.7 1.0 copy-start.7
  162.7 1.4 copy-start.1
  171.0 4.7 %copy-start.4 = (bf16[512,512]{1,0:T(8,128)(2,1)S(1)}, bf16[512,512]{1,0:T(8,128)(2,1)}, u32[]{:S(2)}) copy-start(bf16[512,512]{1,0:T(8,128)(2,1)} %get-tuple-element.27.refs_0_.refs_5_) | copy-start | bytes 1572868
  171.0 57.9 %all-to-all-start.1 = ((bf16[32,40,512]{2,1,0:T(8,128)(2,1)}), bf16[32,40,512]{2,1,0:T(8,128)(2,1)S(1)}, u32[]{:S(2)}, u32[]{:S(2)}) async-start(bf16[32,40,512]{2,1,0:T(8,128)(2,1)} %shard_map.150), calls=%async_computation.1 | async-start | bytes 2621440 | tf_op jit(solution)/shard_map/all_to_all | solution.py:369
  175.7 27.4 %collective-permute-start.13 = (bf16[512,512]{1,0:T(8,128)(2,1)S(1)}, bf16[512,512]{1,0:T(8,128)(2,1)S(1)}, u32[]{:S(2)}, u32[]{:S(2)}) collective-permute-start(bf16[512,512]{1,0:T(8,128)(2,1)S(1)} %copy-done.4), channel_id=1, source_target_pairs={{0,1},{1,0},{2,3},{3,2},{4,5},{5,4},{6,7},{7,6},{8,9},{9,8},{10,11... | collective-permute-start | bytes 1572872 | tf_op jit(solution)/shard_map/ppermute | solution.py:289
  177.3 25.8 %collective-permute-start.14 = (bf16[512,512]{1,0:T(8,128)(2,1)S(1)}, bf16[512,512]{1,0:T(8,128)(2,1)S(1)}, u32[]{:S(2)}, u32[]{:S(2)}) collective-permute-start(bf16[512,512]{1,0:T(8,128)(2,1)S(1)} %copy-done.4), channel_id=1, source_target_pairs={{0,2},{1,3},{2,0},{3,1},{4,6},{5,7},{6,4},{7,5},{8,10},{9,11},{10,... | collective-permute-start | bytes 1572872 | tf_op jit(solution)/shard_map/ppermute | solution.py:289
  178.8 37.4 %collective-permute-start.15 = (bf16[512,512]{1,0:T(8,128)(2,1)S(1)}, bf16[512,512]{1,0:T(8,128)(2,1)S(1)}, u32[]{:S(2)}, u32[]{:S(2)}) collective-permute-start(bf16[512,512]{1,0:T(8,128)(2,1)S(1)} %copy-done.4), channel_id=1, source_target_pairs={{0,3},{1,2},{2,1},{3,0},{4,7},{5,6},{6,5},{7,4},{8,11},{9,10},{10,... | collective-permute-start | bytes 1572872 | tf_op jit(solution)/shard_map/ppermute | solution.py:289
  203.1 13.1 %copy-start.8 = (bf16[512,512]{1,0:T(8,128)(2,1)}, bf16[512,512]{1,0:T(8,128)(2,1)S(1)}, u32[]{:S(2)}) copy-start(bf16[512,512]{1,0:T(8,128)(2,1)S(1)} %collective-permute-done.13.refs_1_) | copy-start | bytes 1572868
  203.1 13.1 %copy-start.9 = (bf16[512,512]{1,0:T(8,128)(2,1)}, bf16[512,512]{1,0:T(8,128)(2,1)S(1)}, u32[]{:S(2)}) copy-start(bf16[512,512]{1,0:T(8,128)(2,1)S(1)} %collective-permute-done.14.refs_2_) | copy-start | bytes 1572868
  216.2 0.8 copy-start.10
  220.7 6.6 %collective-permute-start.16 = (bf16[512,128]{1,0:T(8,128)(2,1)}, bf16[512,128]{1,0:T(8,128)(2,1)S(1)}, u32[]{:S(2)}, u32[]{:S(2)}) collective-permute-start(bf16[512,128]{1,0:T(8,128)(2,1)} %shard_map.149.refs_0_), channel_id=1, source_target_pairs={{0,1},{1,0},{2,3},{3,2},{4,5},{5,4},{6,7},{7,6},{8,9},{9,8},{10,11... | collective-permute-start | bytes 393224 | tf_op jit(solution)/shard_map/ppermute | solution.py:289
  221.2 7.7 %collective-permute-start.17 = (bf16[512,128]{1,0:T(8,128)(2,1)}, bf16[512,128]{1,0:T(8,128)(2,1)S(1)}, u32[]{:S(2)}, u32[]{:S(2)}) collective-permute-start(bf16[512,128]{1,0:T(8,128)(2,1)} %shard_map.149.refs_0_), channel_id=1, source_target_pairs={{0,2},{1,3},{2,0},{3,1},{4,6},{5,7},{6,4},{7,5},{8,10},{9,11},{10,... | collective-permute-start | bytes 393224 | tf_op jit(solution)/shard_map/ppermute | solution.py:289
  221.5 7.4 %collective-permute-start.18 = (bf16[512,128]{1,0:T(8,128)(2,1)}, bf16[512,128]{1,0:T(8,128)(2,1)S(1)}, u32[]{:S(2)}, u32[]{:S(2)}) collective-permute-start(bf16[512,128]{1,0:T(8,128)(2,1)} %shard_map.149.refs_0_), channel_id=1, source_target_pairs={{0,3},{1,2},{2,1},{3,0},{4,7},{5,6},{6,5},{7,4},{8,11},{9,10},{10,... | collective-permute-start | bytes 393224 | tf_op jit(solution)/shard_map/ppermute | solution.py:289
  227.2 1.7 copy-start.24
  228.9 1.1 copy-start
  (7 other events, 5.0 us)
where the time goes:
time: 236 us; the launch traced here: 235 us
  waiting for transfers between devices  142 us (60%)
  Pallas kernels  41.8 us (18%)
  starting transfers between devices  40.2 us (17%)
  local copies, waits for them, and re-layouts  8.37 us (4%)
  other arithmetic  2.9 us (1%)
    ppermute x15, waiting for transfers between devices, over_tp(): return lax.ppermute(x, 'tp', [(i, i ^ k) for i in range(tp)])  120 us
    pallas_call x7, Pallas kernels, call(): pl.pallas_call(kernel, out_shape=out_shape, in_specs=[sm] * smem + [vm] *...  41.8 us
    ppermute x6, waiting for transfers between devices, over_z(): return lax.ppermute(x, 'sp', [(i, i ^ 2 * k) for i in range(sp)])  20.9 us
    ppermute x15, starting transfers between devices, over_tp(): return lax.ppermute(x, 'tp', [(i, i ^ k) for i in range(tp)])  19.1 us
    ppermute x6, starting transfers between devices, over_z(): return lax.ppermute(x, 'sp', [(i, i ^ 2 * k) for i in range(sp)])  11.3 us
    unnamed x56, local copies, waits for them, and re-layouts  5.64 us
  transfers between devices with their start and end apart: 27, of which 14 were waited for; matrix products, arithmetic and copies ran while one was open for 2% of the time, Pallas kernels for 3%

commit v1 on v0

--- a/solution.py
+++ b/solution.py
@@ -13,6 +13,7 @@
 EPSILON = 1e-06
 LOG2E = math.log2(math.e)
 LOW = -1e30
+VMEM_GRANT = 24 * 2**20
 F32 = jnp.float32
 BF16 = jnp.bfloat16
 
@@ -21,16 +22,18 @@
     return jax.nn.silu(gate_part) * up_part
 
 
-def call(kernel, out_shape, args, smem=0, scratch=()):
+def call(kernel, out_shape, args, smem=0, scratch=(), far_in=0):
     vm = pl.BlockSpec(memory_space=pltpu.VMEM)
     sm = pl.BlockSpec(memory_space=pltpu.SMEM)
+    far = pl.BlockSpec(memory_space=pl.ANY)
     single = not isinstance(out_shape, (list, tuple))
     return pl.pallas_call(
         kernel,
         out_shape=out_shape,
-        in_specs=[sm] * smem + [vm] * (len(args) - smem),
+        in_specs=[sm] * smem + [vm] * (len(args) - smem - far_in) + [far] * far_in,
         out_specs=vm if single else [vm] * len(out_shape),
         scratch_shapes=list(scratch),
+        compiler_params=pltpu.CompilerParams(vmem_limit_bytes=None if far_in else VMEM_GRANT),
     )(*args)
 
 
@@ -42,13 +45,44 @@
     return pltpu.roll(x, HDIM, 1)
 
 
-def pack_kernel(heads, z_ref, q_ref, k_ref, v_ref, g_ref, *slabs):
+def cut_copies(sources, sems):
+    copies = []
+    for src, index, dst, cols in sources:
+        dst = dst if cols is None else dst.at[:, cols]
+        copy = pltpu.make_async_copy(src.at[index], dst, sems.at[len(copies)])
+        copy.start()
+        copies.append(copy)
+    return copies
+
+
+def pair_sources(gate_ref, up_ref, index, dst):
+    hid = gate_ref.shape[2]
+    return [(gate_ref, index, dst, slice(0, hid)), (up_ref, index, dst, slice(hid, 2 * hid))]
+
+
+def cut_pairs_kernel(offsets, t_ref, gate_ref, up_ref, *refs):
+    sources = []
+    for offset, dst in zip(offsets, refs[:-1]):
+        sources += pair_sources(gate_ref, up_ref, t_ref[0] ^ offset, dst)
+    for copy in cut_copies(sources, refs[-1]):
+        copy.wait()
+
+
+def cut_downs_kernel(offsets, t_ref, down_ref, *refs):
+    sources = [(down_ref, t_ref[0] ^ offset, dst, None) for offset, dst in zip(offsets, refs[:-1])]
+    for copy in cut_copies(sources, refs[-1]):
+        copy.wait()
+
+
+def pack_kernel(heads, offset, z_ref, t_ref, q_ref, k_ref, v_ref, g_ref, gate_ref, up_ref, down_ref, *refs):
     tok = q_ref.shape[0]
     half = tok // 2
     low = low_lanes((tok, 2 * HDIM))
     low_half = low_lanes((half, 2 * HDIM))
-    o_ref = slabs[-1]
-    slabs = slabs[:-1]
+    slabs, (pair_ref, cut_ref, o_ref, sems) = refs[:heads], refs[heads:]
+    other = t_ref[0] ^ offset
+    sources = pair_sources(gate_ref, up_ref, other, pair_ref) + [(down_ref, other, cut_ref, None)]
+    copies = cut_copies(sources, sems)
     gates = g_ref[...]
     for pair in range(heads // 2):
         cols = slice(pair * 2 * HDIM, (pair + 1) * 2 * HDIM)
@@ -73,15 +107,18 @@
         o_ref[h, tok + half :] = jnp.concatenate(pieces, axis=0).astype(BF16)
     for i, slab in enumerate(slabs):
         slab[...] = o_ref[z_ref[0] ^ i]
-
-
-def attn_kernel(nz, tok, c_ref, z_ref, *refs):
+    for copy in copies:
+        copy.wait()
+
+
+def attn_kernel(nz, tok, ahead, parts, c_ref, z_ref, *refs):
     owns, sws, outs = refs[:nz], refs[nz : 2 * nz], refs[2 * nz : 3 * nz]
     kv_scr, vo_scr, g_scr, q_scr, o_scr = refs[3 * nz :]
     core = c_ref[0]
     half = tok // 2
     wide = 2 * tok
     rows = tok // 128
+    n = half // parts
     low_tok = low_lanes((tok, 128))
     low_half = low_lanes((half, 128))
     for i in range(nz):
@@ -97,44 +134,59 @@
             g = jnp.concatenate([g[r : r + 1] for r in range(rows)], axis=1)
             g_scr[z, 0:1, spot] = g
     scale = HDIM ** (-0.5) * LOG2E
-
-    def step(q, z, state, mask=None):
-        m, acc = state
-        s = lax.dot_general(q, kv_scr[z], (((1,), (1,)), ((), ())), preferred_element_type=F32)
-        t = s * scale - g_scr[z, 0:1]
-        if mask is not None:
-            t = jnp.where(mask, t, LOW)
-        top = jnp.maximum(m, jnp.max(t, axis=1, keepdims=True))
-        p = jnp.exp2(t - top)
-        acc = acc * jnp.exp2(m - top) + jnp.dot(p.astype(BF16), vo_scr[z], preferred_element_type=F32)
-        return top, acc
-
-    key_at = lax.broadcasted_iota(jnp.int32, (half, wide), 1)
-    row_at = lax.broadcasted_iota(jnp.int32, (half, wide), 0) + core * tok
-
-    def one_block(zq, carry):
-        packed = q_scr[zq].astype(F32)
-        qs = (
-            jnp.where(low_half, packed, 0.0).astype(BF16),
-            jnp.where(low_half, swap_halves(packed), 0.0).astype(BF16),
-        )
-        start = tuple((jnp.full((half, 1), LOW, F32), jnp.zeros((half, 128), F32)) for _ in qs)
-        state = lax.fori_loop(0, zq, lambda z, st: tuple(step(q, z, s) for q, s in zip(qs, st)), start)
-        state = tuple(
-            step(q, zq, s, key_at <= row_at + i * half) for i, (q, s) in enumerate(zip(qs, state))
-        )
-        acc_a, acc_b = state[0][1], state[1][1]
-        out_a = swap_halves(acc_a) / acc_a
-        out_b = acc_b / swap_halves(acc_b)
-        o_scr[zq] = jnp.where(low_half, out_a, out_b).astype(BF16)
-        return carry
-
-    lax.fori_loop(0, nz, one_block, 0)
+    key_at = lax.broadcasted_iota(jnp.int32, (n, wide), 1)
+    row_at = lax.broadcasted_iota(jnp.int32, (n, wide), 0) + core * tok
+    low = low_lanes((n, 128))
+    queries = {}
+    state = {}
+
+    def query(zq, i):
+        if zq not in queries:
+            packed = q_scr[zq].astype(F32)
+            queries[zq] = (
+                jnp.where(low_half, packed, 0.0).astype(BF16),
+                jnp.where(low_half, swap_halves(packed), 0.0).astype(BF16),
+            )
+        return queries[zq][i]
+
+    def seen(zq, z, i, p):
+        return wide if z < zq else tok + i * half + (p + 1) * n
+
+    def score(zq, z, i, p):
+        keys = kv_scr[z, 0 : seen(zq, z, i, p)]
+        q = query(zq, i)[p * n : (p + 1) * n]
+        return lax.dot_general(q, keys, (((1,), (1,)), ((), ())), preferred_element_type=F32)
+
+    def absorb(zq, z, i, p, s):
+        keys = seen(zq, z, i, p)
+        t = s * scale - g_scr[z, 0:1, 0:keys]
+        if z == zq:
+            t = jnp.where(key_at[:, :keys] <= row_at[:, :keys] + (i * half + p * n), t, LOW)
+        top = jnp.max(t, axis=1, keepdims=True)
+        if z > 0:
+            m, acc = state[zq, i, p]
+            top = jnp.maximum(m, top)
+        weight = jnp.exp2(t - top).astype(BF16)
+        new = jnp.dot(weight, vo_scr[z, 0:keys], preferred_element_type=F32)
+        if z > 0:
+            new = new + acc * jnp.exp2(m - top)
+        state[zq, i, p] = top, new
+        if z == zq and i == 1:
+            first = state[zq, 0, p][1]
+            out = jnp.where(low, swap_halves(first) / first, new / swap_halves(new))
+            o_scr[zq, p * n : (p + 1) * n] = out.astype(BF16)
+
+    tasks = [(zq, z, i, p) for zq in range(nz) for z in range(zq + 1) for i in range(2) for p in range(parts)]
+    scores = [score(*task) for task in tasks[:ahead]]
+    for at, task in enumerate(tasks):
+        if at + ahead < len(tasks):
+            scores.append(score(*tasks[at + ahead]))
+        absorb(*task, scores.pop(0))
     for i in range(nz):
         outs[i][...] = o_scr[z_ref[0] ^ i]
 
 
-def route_kernel(experts, cap, rt_ref, d_ref, c0_ref, c1_ref):
+def route_kernel(experts, cap, rt_ref, w_ref, d_ref, c_ref):
     tok = rt_ref.shape[1]
     slots = experts * cap
     at = lax.broadcasted_iota(jnp.int32, (tok, tok), 0)
@@ -148,10 +200,11 @@
     sid = lax.broadcasted_iota(jnp.int32, (slots, tok), 0)
     d_ref[...] = jnp.where((sid == rows[0]) | (sid == rows[1]), 1.0, 0.0).astype(BF16)
     cols = jnp.concatenate([r.astype(F32) for r in rows] * 4, axis=0).T.astype(jnp.int32)
+    w = jnp.concatenate([w_ref[...]] * 4, axis=0).T
     cols = [cols[:, k : k + 1] for k in range(2)]
     sid = lax.broadcasted_iota(jnp.int32, (tok, slots), 1)
-    c0_ref[...] = jnp.where(sid == cols[0], 1.0, 0.0).astype(BF16)
-    c1_ref[...] = jnp.where(sid == cols[1], 1.0, 0.0).astype(BF16)
+    mix = jnp.where(sid == cols[0], w[:, 0:1], jnp.where(sid == cols[1], w[:, 1:2], 0.0))
+    c_ref[...] = mix.astype(BF16)
 
 
 def mid_kernel(heads, cap, t_ref, z_ref, *refs):
@@ -195,12 +248,14 @@
 
 
 def shared_kernel(t_ref, *refs):
-    n = len(refs) - 4
-    parts, (gain_ref, gate_ref, up_ref, o_ref) = refs[:n], refs[n:]
+    n = len(refs) - 5
+    parts, halves, (gain_ref, gate_ref, up_ref, o_ref) = refs[: n - 1], refs[n - 1 : n + 1], refs[n + 1 :]
     part_width = parts[0].shape[1]
     width = n * part_width
     srcs = [t_ref[0] ^ k for k in range(n)]
-    normed = normed_of([p[...].astype(F32) for p in parts], [gain_ref[s] for s in srcs], width)
+    rows = [p[...].astype(F32) for p in parts]
+    rows.append(jnp.concatenate([h[...].astype(F32) for h in halves], axis=0))
+    normed = normed_of(rows, [gain_ref[s] for s in srcs], width)
     both = None
     for s, x in zip(srcs, normed):
         rows = pl.ds(pl.multiple_of(s * part_width, part_width), part_width)
@@ -235,22 +290,22 @@
             y_ref[s * tp + (me ^ k)] = y[s * cap : (s + 1) * cap].astype(BF16)
 
 
+def picks_kernel(mid_ref, ret_ref, c_ref, o_ref):
+    experts, cap, width = ret_ref.shape
+    rows = ret_ref[...].astype(F32).reshape(experts * cap, width).astype(BF16)
+    o_ref[...] = mid_ref[...].astype(F32) + jnp.dot(c_ref[...], rows, preferred_element_type=F32)
+
+
 def final_kernel(t_ref, *refs):
-    n = len(refs) - 8
+    n = len(refs) - 4
     hids = refs[:n]
-    down_ref, mid_ref, ret_ref, c0_ref, c1_ref, w_ref, o_ref, h_scr = refs[n:]
+    down_ref, sum_ref, o_ref, h_scr = refs[n:]
     hid = hids[0].shape[1]
     for k in range(n):
         spot = pl.ds(pl.multiple_of((t_ref[0] ^ k) * hid, hid), hid)
         h_scr[:, spot] = hids[k][...]
     out = jnp.dot(h_scr[...], down_ref[...], preferred_element_type=F32)
-    experts, cap, width = ret_ref.shape
-    rows = ret_ref[...].astype(F32).reshape(experts * cap, width).astype(BF16)
-    out = out + mid_ref[...].astype(F32)
-    w = jnp.concatenate([w_ref[...]] * 4, axis=0).T
-    out = out + w[:, 0:1] * jnp.dot(c0_ref[...], rows, preferred_element_type=F32)
-    out = out + w[:, 1:2] * jnp.dot(c1_ref[...], rows, preferred_element_type=F32)
-    o_ref[...] = out.astype(BF16)
+    o_ref[...] = (sum_ref[...] + out).astype(BF16)
 
 
 def shards(
@@ -297,40 +352,54 @@
     def over_z(x, k):
         return lax.ppermute(x, "sp", [(i, i ^ (2 * k)) for i in range(sp)])
 
-    slabs = call(
-        functools.partial(pack_kernel, heads),
-        [jax.ShapeDtypeStruct((rows, 128), BF16)] * heads,
-        (z_ref, queries, key_vectors, value_vectors, log_gate_sums.T),
-        smem=1,
-        scratch=(pltpu.VMEM((heads, rows, 128), BF16),),
+    pair_shape = jax.ShapeDtypeStruct((expert_gate.shape[1], 2 * expert_gate.shape[2]), BF16)
+    down_shape = jax.ShapeDtypeStruct(expert_down.shape[1:], BF16)
+    *slabs, far_pair, far_down = call(
+        functools.partial(pack_kernel, heads, tp - 1),
+        [jax.ShapeDtypeStruct((rows, 128), BF16)] * heads + [pair_shape, down_shape],
+        (z_ref, me_ref, queries, key_vectors, value_vectors, log_gate_sums.T)
+        + (expert_gate, expert_up, expert_down),
+        smem=2,
+        scratch=(pltpu.VMEM((heads, rows, 128), BF16), pltpu.SemaphoreType.DMA((3,))),
+        far_in=3,
     )
     owns = [slabs[0]] + [over_z(slabs[k], k) for k in range(1, nz)]
     swapped = [lax.ppermute(x, "sp", [(i, i ^ 1) for i in range(sp)]) for x in owns]
 
-    def deal(pieces):
-        return pieces[:1] + [over_tp(pieces[k], k) for k in range(1, tp)]
-
-    def pick(weights, k):
-        return lax.dynamic_index_in_dim(weights, me ^ k, 0, keepdims=False)
-
-    pairs = deal(
-        [jnp.concatenate([pick(expert_gate, k), pick(expert_up, k)], axis=1) for k in range(tp)]
-    )
-    downs = deal([pick(expert_down, k) for k in range(tp)])
-
-    spread, pick0, pick1 = call(
+    near = tuple(range(tp - 1))
+    near_downs = call(
+        functools.partial(cut_downs_kernel, near),
+        [down_shape] * len(near),
+        (me_ref, expert_down),
+        smem=1,
+        scratch=(pltpu.SemaphoreType.DMA((len(near),)),),
+        far_in=1,
+    )
+    near_pairs = call(
+        functools.partial(cut_pairs_kernel, near),
+        [pair_shape] * len(near),
+        (me_ref, expert_gate, expert_up),
+        smem=1,
+        scratch=(pltpu.SemaphoreType.DMA((2 * len(near),)),),
+        far_in=2,
+    )
+    pairs = [near_pairs[0]] + [over_tp(near_pairs[k], k) for k in near[1:]]
+    downs = [near_downs[0]] + [over_tp(near_downs[k], k) for k in near[1:]]
+    pairs.append(over_tp(far_pair, tp - 1))
+    downs.append(over_tp(far_down, tp - 1))
+
+    spread, mix = call(
         functools.partial(route_kernel, experts, cap),
         [
             jax.ShapeDtypeStruct((experts * cap, tok), BF16),
             jax.ShapeDtypeStruct((tok, experts * cap), BF16),
-            jax.ShapeDtypeStruct((tok, experts * cap), BF16),
         ],
-        (routes.T,),
+        (routes.T, route_weight.T),
     )
     gain = norm_gain.astype(F32).reshape(tp, 1, width)
 
     mixed = call(
-        functools.partial(attn_kernel, nz, tok),
+        functools.partial(attn_kernel, nz, tok, 2, 2),
         [jax.ShapeDtypeStruct((half, 128), BF16)] * nz,
         (core_ref, z_ref, *owns, *swapped),
         smem=2,
@@ -355,7 +424,8 @@
         smem=2,
     )
     arrived = lax.all_to_all(outgoing, ("sp", "tp"), 0, 0, tiled=True)
-    mids = all_tp(mid)
+    mids = [mid] + [over_tp(mid, k) for k in range(1, tp - 1)]
+    mids += [over_tp(mids[2][:half], 1), over_tp(mids[1][half:], 2)]
     produced = call(
         functools.partial(expert_kernel, sp, tp),
         jax.ShapeDtypeStruct((sp * tp, cap, width), BF16),
@@ -374,10 +444,11 @@
         smem=1,
     )
     shared_mids = all_tp(shared_mid)
+    summed = call(picks_kernel, jax.ShapeDtypeStruct((tok, width), F32), (mid, returned, mix))
     return call(
         final_kernel,
         jax.ShapeDtypeStruct((tok, width), BF16),
-        (me_ref, *shared_mids, shared_down, mid, returned, pick0, pick1, route_weight.T),
+        (me_ref, *shared_mids, shared_down, summed),
         smem=1,
         scratch=(pltpu.VMEM((tok, shared_down.shape[0]), BF16),),
     )
@@ -564,7 +635,7 @@
     def program(*args):
         heads = args[3].shape[1] // tp
         exp_dev = args[9].shape[0] // sp
-        deals = sp % 2 == 0 and heads * 2 == sp and exp_dev == tp and tp & (tp - 1) == 0
+        deals = sp % 2 == 0 and heads * 2 == sp and exp_dev == tp and tp == 4
         body = layer if deals else generic_shards
         mapped = jax.shard_map(body, mesh=mesh, in_specs=placed, out_specs=P("sp", "tp"), check_vma=False)
         return mapped(*args)

time: 236 us -> 218 us (0.924)
  Pallas kernels: 41.8 us -> 31 us
  waiting for transfers between devices: 142 us -> 136 us
  other arithmetic: 2.9 us -> 0.04 us
    pallas_call x7 -> x10, Pallas kernels: 41.8 us -> 31 us  [call(): pl.pallas_call(kernel, out_shape=out_shape, in_specs=[sm] * smem + [vm] *...]
    ppermute x15 -> x16, waiting for transfers between devices: 120 us -> 114 us  [over_tp(): return lax.ppermute(x, 'tp', [(i, i ^ k) for i in range(tp)])]
    squeeze x2 -> x0, local copies, waits for them, and re-layouts: 2.73 us -> none  [pick(): return lax.dynamic_index_in_dim(weights, me ^ k, 0, keepdims=False)]
    unnamed x56 -> x32, local copies, waits for them, and re-layouts: 5.64 us -> 8 us
    ppermute x15 -> x16, starting transfers between devices: 19.1 us -> 20.4 us  [over_tp(): return lax.ppermute(x, 'tp', [(i, i ^ k) for i in range(tp)])]
  transfers between devices with their start and end apart: 27 -> 28, of which waited for: 14 -> 14; matrix products, arithmetic and copies ran while one was open for 2% -> 0% of each run, Pallas kernels for 3% -> 5%
where the time goes in v1:
time: 218 us; the launch traced here: 217 us
  waiting for transfers between devices  136 us (62%)
  starting transfers between devices  41.7 us (19%)
  Pallas kernels  31 us (14%)
  local copies, waits for them, and re-layouts  8.04 us (4%)
    ppermute x16, waiting for transfers between devices, over_tp(): return lax.ppermute(x, 'tp', [(i, i ^ k) for i in range(tp)])  114 us
    pallas_call x10, Pallas kernels, call(): pl.pallas_call(kernel, out_shape=out_shape, in_specs=[sm] * smem + [vm] *...  31 us
    ppermute x6, waiting for transfers between devices, over_z(): return lax.ppermute(x, 'sp', [(i, i ^ 2 * k) for i in range(sp)])  20.7 us
    ppermute x16, starting transfers between devices, over_tp(): return lax.ppermute(x, 'tp', [(i, i ^ k) for i in range(tp)])  20.4 us
    ppermute x6, starting transfers between devices, over_z(): return lax.ppermute(x, 'sp', [(i, i ^ 2 * k) for i in range(sp)])  11.4 us
    unnamed x32, local copies, waits for them, and re-layouts  8 us
    all_to_all x1, starting transfers between devices, shards(): returned = lax.all_to_all(produced, ('sp', 'tp'), 0, 0, tiled=True)  4.73 us
    all_to_all x1, starting transfers between devices, shards(): arrived = lax.all_to_all(outgoing, ('sp', 'tp'), 0, 0, tiled=True)  4.58 us
  transfers between devices with their start and end apart: 28, of which 14 were waited for; matrix products, arithmetic and copies ran while one was open for 0% of the time, Pallas kernels for 5%

profile of v1, /device:TPU:0, one launch (start us, length us, event | category | flops | bytes accessed | tf_op | source)
XLA Modules:
  0.0 217.4 jit_solution(4861238126391327599)
XLA Ops:
  0.0 3.9 %shard_map.145 = (bf16[784,128]{1,0:T(8,128)(2,1)}, bf16[784,128]{1,0:T(8,128)(2,1)}, bf16[784,128]{1,0:T(8,128)(2,1)}, bf16[784,128]{1,0:T(8,128)(2,1)}, bf16[2...) custom-call(s32[1]{0:T(128)} %bitcast.1.z_ref, s32[1]{0:T(128)} %bitcast.t_ref, bf16[512,256]{1,0:T(8,128)(2,1)} %q_ref.1, ...), custom_call_target="tpu_custom_call" | custom-call | tf_op jit(solution)/shard_map/pallas_call | solution.py:30
  4.0 3.1 %collective-permute-start = (bf16[784,128]{1,0:T(8,128)(2,1)}, bf16[784,128]{1,0:T(8,128)(2,1)S(1)}, u32[]{:S(2)}, u32[]{:S(2)}) collective-permute-start(bf16[784,128]{1,0:T(8,128)(2,1)} %get-tuple-element.26), channel_id=1, source_target_pairs={{0,8},{4,12},{8,0},{12,4},{16,24},{20,28},{24,16},{28,20},{1,9},{5... | collective-permute-start | bytes 602120 | tf_op jit(solution)/shard_map/ppermute | solution.py:353
  7.1 2.6 %collective-permute-start.1 = (bf16[784,128]{1,0:T(8,128)(2,1)}, bf16[784,128]{1,0:T(8,128)(2,1)S(1)}, u32[]{:S(2)}, u32[]{:S(2)}) collective-permute-start(bf16[784,128]{1,0:T(8,128)(2,1)} %get-tuple-element.27), channel_id=1, source_target_pairs={{0,16},{4,20},{8,24},{12,28},{16,0},{20,4},{24,8},{28,12},{1,17},{... | collective-permute-start | bytes 602120 | tf_op jit(solution)/shard_map/ppermute | solution.py:353
  9.7 6.2 %collective-permute-done.refs_1_ = bf16[784,128]{1,0:T(8,128)(2,1)S(1)} collective-permute-done((bf16[784,128]{1,0:T(8,128)(2,1)}, bf16[784,128]{1,0:T(8,128)(2,1)S(1)}, u32[]{:S(2)}, u32[]{:S(2)}) %collective-permute-start) | collective-permute-done | bytes 200736 | tf_op jit(solution)/shard_map/ppermute | solution.py:353
  15.8 8.8 %collective-permute-done.1.refs_2_ = bf16[784,128]{1,0:T(8,128)(2,1)S(1)} collective-permute-done((bf16[784,128]{1,0:T(8,128)(2,1)}, bf16[784,128]{1,0:T(8,128)(2,1)S(1)}, u32[]{:S(2)}, u32[]{:S(2)}) %collective-permute-start.1) | collective-permute-done | bytes 200736 | tf_op jit(solution)/shard_map/ppermute | solution.py:353
  25.2 0.9 collective-permute-done.5.refs_6_
  26.4 0.9 copy-done.12
  27.3 7.1 %shard_map.146 = (bf16[256,128]{1,0:T(8,128)(2,1)S(1)}, bf16[256,128]{1,0:T(8,128)(2,1)S(1)}, bf16[256,128]{1,0:T(8,128)(2,1)S(1)}, bf16[256,128]{1,0:T(8,128)(2,1)S(1)}) custom-call(s32[1]{0:T(128)} %bitcast.2.c_ref, s32[1]{0:T(128)} %bitcast.1.z_ref, bf16[784,128]{1,0:T(8,128)(2,1)S(1)} %copy-done.12, bf16[784,128]{1,0:T(8,128)(2,1)S(1)} %collective-permute-done.refs_1_, ...), custom_call_target="tpu_custom_call" | custom-call | tf_op jit(solution)/shard_map/pallas_call | solution.py:30
  34.4 3.3 %collective-permute-start.7 = (bf16[256,128]{1,0:T(8,128)(2,1)S(1)}, bf16[256,128]{1,0:T(8,128)(2,1)S(1)}, u32[]{:S(2)}, u32[]{:S(2)}) collective-permute-start(bf16[256,128]{1,0:T(8,128)(2,1)S(1)} %get-tuple-element.30), channel_id=1, source_target_pairs={{0,8},{4,12},{8,0},{12,4},{16,24},{20,28},{24,16},{28,20},{1,9},{5... | collective-permute-start | bytes 196616 | tf_op jit(solution)/shard_map/ppermute | solution.py:353
  37.7 1.1 collective-permute-start.8
  38.8 1.4 collective-permute-start.9
  40.2 5.8 %collective-permute-done.8 = bf16[256,128]{1,0:T(8,128)(2,1)S(1)} collective-permute-done((bf16[256,128]{1,0:T(8,128)(2,1)S(1)}, bf16[256,128]{1,0:T(8,128)(2,1)S(1)}, u32[]{:S(2)}, u32[]{:S(2)}) %collective-permute-start.8) | collective-permute-done | bytes 65568 | tf_op jit(solution)/shard_map/ppermute | solution.py:353
  46.0 1.5 collective-permute-start.10
  47.5 1.5 collective-permute-start.11
  49.5 2.2 %shard_map.147 = (bf16[1280,512]{1,0:T(8,128)(2,1)S(1)}, bf16[512,1280]{1,0:T(8,128)(2,1)S(1)}) custom-call(s32[2,512]{1,0:T(2,128)S(1)} %bitcast.14, f32[2,512]{1,0:T(2,128)S(1)} %bitcast.15), custom_call_target="tpu_custom_call" | custom-call | tf_op jit(solution)/shard_map/pallas_call | solution.py:30
  51.7 3.5 %collective-permute-done.10.refs_1_ = bf16[4,256,128]{2,1,0:T(8,128)(2,1)S(1)} collective-permute-done((bf16[4,256,128]{2,1,0:T(8,128)(2,1)S(1)}, bf16[4,256,128]{2,1,0:T(8,128)(2,1)S(1)}, u32[]{:S(2)}, u32[]{:S(2)}) %collective-permute-start.10) | collective-permute-done | bytes 262176 | tf_op jit(solution)/shard_map/ppermute | solution.py:344
  55.2 4.5 %collective-permute-done.11.refs_2_ = bf16[4,256,128]{2,1,0:T(8,128)(2,1)S(1)} collective-permute-done((bf16[4,256,128]{2,1,0:T(8,128)(2,1)S(1)}, bf16[4,256,128]{2,1,0:T(8,128)(2,1)S(1)}, u32[]{:S(2)}, u32[]{:S(2)}) %collective-permute-start.11) | collective-permute-done | bytes 262176 | tf_op jit(solution)/shard_map/ppermute | solution.py:344
  59.7 1.8 shard_map.148
  61.5 1.1 copy-done
  62.6 4.6 %all-to-all-start = ((bf16[32,40,512]{2,1,0:T(8,128)(2,1)}), bf16[32,40,512]{2,1,0:T(8,128)(2,1)S(1)}, u32[]{:S(2)}, u32[]{:S(2)}) async-start(bf16[32,40,512]{2,1,0:T(8,128)(2,1)} %copy-done), calls=%async_computation | async-start | bytes 2621440 | tf_op jit(solution)/shard_map/all_to_all | solution.py:426
  67.2 2.7 %collective-permute-start.22 = (bf16[2048,256]{1,0:T(8,128)(2,1)}, bf16[2048,256]{1,0:T(8,128)(2,1)}, u32[]{:S(2)}, u32[]{:S(2)}) collective-permute-start(bf16[2048,256]{1,0:T(8,128)(2,1)} %get-tuple-element.39), channel_id=1, source_target_pairs={{0,3},{1,2},{2,1},{3,0},{4,7},{5,6},{6,5},{7,4},{8,11},{9,10},{10,... | collective-permute-start | bytes 3145736 | tf_op jit(solution)/shard_map/ppermute | solution.py:344
  70.2 3.6 %shard_map.150 = (bf16[2048,256]{1,0:T(8,128)(2,1)}, bf16[2048,256]{1,0:T(8,128)(2,1)}, bf16[2048,256]{1,0:T(8,128)(2,1)}) custom-call(s32[1]{0:T(128)} %bitcast.t_ref, bf16[4,2048,128]{2,1,0:T(8,128)(2,1)} %gate_ref.3, bf16[4,2048,128]{2,1,0:T(8,128)(2,1)} %up_ref.3), custom_call_target="tpu_custom_call" | custom-call | tf_op jit(solution)/shard_map/pallas_call | solution.py:30
  73.8 1.8 collective-permute-start.20
  75.6 1.5 collective-permute-start.21
  77.1 2.5 %shard_map.151 = (bf16[512,512]{1,0:T(8,128)(2,1)}, bf16[512,512]{1,0:T(8,128)(2,1)}, bf16[512,512]{1,0:T(8,128)(2,1)}) custom-call(s32[1]{0:T(128)} %bitcast.t_ref, bf16[4,512,512]{2,1,0:T(8,128)(2,1)} %down_ref.3), custom_call_target="tpu_custom_call" | custom-call | tf_op jit(solution)/shard_map/pallas_call | solution.py:30
  80.3 40.3 %collective-permute-done.25.refs_7_ = bf16[512,512]{1,0:T(8,128)(2,1)} collective-permute-done((bf16[512,512]{1,0:T(8,128)(2,1)}, bf16[512,512]{1,0:T(8,128)(2,1)}, u32[]{:S(2)}, u32[]{:S(2)}) %collective-permute-start.25) | collective-permute-done | bytes 524320 | tf_op jit(solution)/shard_map/ppermute | solution.py:344
  120.6 0.6 collective-permute-start.24
  121.2 31.6 %collective-permute-done.23.refs_5_ = bf16[512,512]{1,0:T(8,128)(2,1)S(1)} collective-permute-done((bf16[512,512]{1,0:T(8,128)(2,1)}, bf16[512,512]{1,0:T(8,128)(2,1)S(1)}, u32[]{:S(2)}, u32[]{:S(2)}) %collective-permute-start.23) | collective-permute-done | bytes 524320 | tf_op jit(solution)/shard_map/ppermute | solution.py:344
  152.8 0.8 copy-done.8
  153.6 0.8 copy-done.10
  154.4 1.2 copy-done.2
  155.6 1.0 copy-done.7
  156.7 1.0 copy-done.9
  157.7 1.0 copy-done.11
  158.8 5.7 %shard_map.152 = bf16[32,40,512]{2,1,0:T(8,128)(2,1)} custom-call(s32[1]{0:T(128)} %bitcast.t_ref, bf16[32,40,512]{2,1,0:T(8,128)(2,1)S(1)} %all-to-all-done.x_ref, f32[4,1,512]{2,1,0:T(1,128)S(1)} %bitcast.11, bf16[2048,256]{1,0:T(8,128)(2,1)S(1)} %copy-done.2, bf16[2048,256]{1,0:T(8,128)(2,1)} %collective-permute-done.20.refs_1_, ...), custom_call_target="tpu_custom_call" | custom-call | tf_op jit(solution)/shard_map/pallas_call | solution.py:30
  164.5 4.7 %all-to-all-start.1 = ((bf16[32,40,512]{2,1,0:T(8,128)(2,1)}), bf16[32,40,512]{2,1,0:T(8,128)(2,1)S(1)}, u32[]{:S(2)}, u32[]{:S(2)}) async-start(bf16[32,40,512]{2,1,0:T(8,128)(2,1)} %shard_map.152), calls=%async_computation.1 | async-start | bytes 2621440 | tf_op jit(solution)/shard_map/all_to_all | solution.py:439
  169.2 1.8 collective-permute-start.14
  171.1 1.5 collective-permute-start.13
  172.5 23.0 %collective-permute-done.14.refs_2_ = bf16[512,512]{1,0:T(8,128)(2,1)S(1)} collective-permute-done((bf16[512,512]{1,0:T(8,128)(2,1)S(1)}, bf16[512,512]{1,0:T(8,128)(2,1)S(1)}, u32[]{:S(2)}, u32[]{:S(2)}) %collective-permute-start.14) | collective-permute-done | bytes 524320 | tf_op jit(solution)/shard_map/ppermute | solution.py:344
  195.6 2.0 collective-permute-start.15
  198.1 6.3 %collective-permute-done.15.refs_3_ = bf16[256,512]{1,0:T(8,128)(2,1)S(1)} collective-permute-done((bf16[256,512]{1,0:T(8,128)(2,1)S(1)}, bf16[256,512]{1,0:T(8,128)(2,1)S(1)}, u32[]{:S(2)}, u32[]{:S(2)}) %collective-permute-start.15) | collective-permute-done | bytes 262176 | tf_op jit(solution)/shard_map/ppermute | solution.py:344
  204.4 1.8 collective-permute-done.16.refs_4_
  206.2 1.1 shard_map.149.refs_0_
  207.8 3.0 %collective-permute-start.19 = (bf16[512,128]{1,0:T(8,128)(2,1)S(1)}, bf16[512,128]{1,0:T(8,128)(2,1)}, u32[]{:S(2)}, u32[]{:S(2)}) collective-permute-start(bf16[512,128]{1,0:T(8,128)(2,1)S(1)} %shard_map.149.refs_0_), channel_id=1, source_target_pairs={{0,3},{1,2},{2,1},{3,0},{4,7},{5,6},{6,5},{7,4},{8,11},{9,10},{10,... | collective-permute-start | bytes 393224 | tf_op jit(solution)/shard_map/ppermute | solution.py:344
  210.9 0.8 shard_map.153.refs_5_
  211.7 1.9 collective-permute-done.17.refs_1_
  213.7 1.5 collective-permute-done.18.refs_2_
  215.2 2.2 %shard_map.154 = bf16[512,512]{1,0:T(8,128)(2,1)} custom-call(s32[1]{0:T(128)} %bitcast.t_ref, bf16[512,128]{1,0:T(8,128)(2,1)S(1)} %shard_map.149.refs_0_, bf16[512,128]{1,0:T(8,128)(2,1)S(1)} %collective-permute-done.17.refs_1_, bf16[512,128]{1,0:T(8,128)(2,1)S(1)} %collective-permute-done.18.refs_2_, bf16[512,128]{1,0:T(8,128)(2,1)} %collective-permute-done.19.refs_3_, ...), custom_call_target="tpu_custom_call" | custom-call | tf_op jit(solution)/shard_map/pallas_call | solution.py:30
  (54 shorter events, 3.3 us)
Async XLA Ops:
  0.0 49.5 %copy-start.13 = (s32[512,2]{0,1:T(2,128)S(1)}, s32[512,2]{0,1:T(2,128)}, u32[]{:S(2)}) copy-start(s32[512,2]{0,1:T(2,128)} %param.22) | copy-start | bytes 12292
  0.0 49.5 %copy-start.14 = (f32[512,2]{0,1:T(2,128)S(1)}, f32[512,2]{0,1:T(2,128)}, u32[]{:S(2)}) copy-start(f32[512,2]{0,1:T(2,128)} %param.23) | copy-start | bytes 12292
  3.9 55.8 %copy-start.1 = (bf16[1024,512]{1,0:T(8,128)(2,1)S(1)}, bf16[1024,512]{1,0:T(8,128)(2,1)}, u32[]{:S(2)}) copy-start(bf16[1024,512]{1,0:T(8,128)(2,1)} %refs_4_.2) | copy-start | bytes 3145732
  3.9 55.8 %copy-start.3 = (bf16[512,512]{1,0:T(8,128)(2,1)S(1)}, bf16[512,512]{1,0:T(8,128)(2,1)}, u32[]{:S(2)}) copy-start(bf16[512,512]{1,0:T(8,128)(2,1)} %refs_5_.1) | copy-start | bytes 1572868
  4.0 11.9 %collective-permute-start = (bf16[784,128]{1,0:T(8,128)(2,1)}, bf16[784,128]{1,0:T(8,128)(2,1)S(1)}, u32[]{:S(2)}, u32[]{:S(2)}) collective-permute-start(bf16[784,128]{1,0:T(8,128)(2,1)} %get-tuple-element.26), channel_id=1, source_target_pairs={{0,8},{4,12},{8,0},{12,4},{16,24},{20,28},{24,16},{28,20},{1,9},{5... | collective-permute-start | bytes 602120 | tf_op jit(solution)/shard_map/ppermute | solution.py:353
  7.1 17.6 %collective-permute-start.1 = (bf16[784,128]{1,0:T(8,128)(2,1)}, bf16[784,128]{1,0:T(8,128)(2,1)S(1)}, u32[]{:S(2)}, u32[]{:S(2)}) collective-permute-start(bf16[784,128]{1,0:T(8,128)(2,1)} %get-tuple-element.27), channel_id=1, source_target_pairs={{0,16},{4,20},{8,24},{12,28},{16,0},{20,4},{24,8},{28,12},{1,17},{... | collective-permute-start | bytes 602120 | tf_op jit(solution)/shard_map/ppermute | solution.py:353
  9.7 15.0 %collective-permute-start.2 = (bf16[784,128]{1,0:T(8,128)(2,1)}, bf16[784,128]{1,0:T(8,128)(2,1)S(1)}, u32[]{:S(2)}, u32[]{:S(2)}) collective-permute-start(bf16[784,128]{1,0:T(8,128)(2,1)} %get-tuple-element.28), channel_id=1, source_target_pairs={{0,24},{4,28},{8,16},{12,20},{16,8},{20,12},{24,0},{28,4},{1,25},{... | collective-permute-start | bytes 602120 | tf_op jit(solution)/shard_map/ppermute | solution.py:353
  9.7 15.5 %collective-permute-start.3 = (bf16[784,128]{1,0:T(8,128)(2,1)}, bf16[784,128]{1,0:T(8,128)(2,1)S(1)}, u32[]{:S(2)}, u32[]{:S(2)}) collective-permute-start(bf16[784,128]{1,0:T(8,128)(2,1)} %get-tuple-element.25.refs_0_), channel_id=1, source_target_pairs={{0,4},{4,0},{8,12},{12,8},{16,20},{20,16},{24,28},{28,24},{1,5},{5... | collective-permute-start | bytes 602120 | tf_op jit(solution)/shard_map/ppermute | solution.py:367
  15.8 9.3 %collective-permute-start.4 = (bf16[784,128]{1,0:T(8,128)(2,1)S(1)}, bf16[784,128]{1,0:T(8,128)(2,1)S(1)}, u32[]{:S(2)}, u32[]{:S(2)}) collective-permute-start(bf16[784,128]{1,0:T(8,128)(2,1)S(1)} %collective-permute-done.refs_1_), channel_id=1, source_target_pairs={{0,4},{4,0},{8,12},{12,8},{16,20},{20,16},{24,28},{28,24},{1,5},{5... | collective-permute-start | bytes 602120 | tf_op jit(solution)/shard_map/ppermute | solution.py:367
  24.7 1.4 collective-permute-start.5
  24.7 1.7 collective-permute-start.6
  26.4 0.9 copy-start.12
  34.4 5.7 %collective-permute-start.7 = (bf16[256,128]{1,0:T(8,128)(2,1)S(1)}, bf16[256,128]{1,0:T(8,128)(2,1)S(1)}, u32[]{:S(2)}, u32[]{:S(2)}) collective-permute-start(bf16[256,128]{1,0:T(8,128)(2,1)S(1)} %get-tuple-element.30), channel_id=1, source_target_pairs={{0,8},{4,12},{8,0},{12,4},{16,24},{20,28},{24,16},{28,20},{1,9},{5... | collective-permute-start | bytes 196616 | tf_op jit(solution)/shard_map/ppermute | solution.py:353
  37.7 8.2 %collective-permute-start.8 = (bf16[256,128]{1,0:T(8,128)(2,1)S(1)}, bf16[256,128]{1,0:T(8,128)(2,1)S(1)}, u32[]{:S(2)}, u32[]{:S(2)}) collective-permute-start(bf16[256,128]{1,0:T(8,128)(2,1)S(1)} %get-tuple-element.31), channel_id=1, source_target_pairs={{0,16},{4,20},{8,24},{12,28},{16,0},{20,4},{24,8},{28,12},{1,17},{... | collective-permute-start | bytes 196616 | tf_op jit(solution)/shard_map/ppermute | solution.py:353
  38.8 7.1 %collective-permute-start.9 = (bf16[256,128]{1,0:T(8,128)(2,1)S(1)}, bf16[256,128]{1,0:T(8,128)(2,1)S(1)}, u32[]{:S(2)}, u32[]{:S(2)}) collective-permute-start(bf16[256,128]{1,0:T(8,128)(2,1)S(1)} %get-tuple-element.32), channel_id=1, source_target_pairs={{0,24},{4,28},{8,16},{12,20},{16,8},{20,12},{24,0},{28,4},{1,25},{... | collective-permute-start | bytes 196616 | tf_op jit(solution)/shard_map/ppermute | solution.py:353
  46.0 9.2 %collective-permute-start.10 = (bf16[4,256,128]{2,1,0:T(8,128)(2,1)S(1)}, bf16[4,256,128]{2,1,0:T(8,128)(2,1)S(1)}, u32[]{:S(2)}, u32[]{:S(2)}) collective-permute-start(bf16[4,256,128]{2,1,0:T(8,128)(2,1)S(1)} %pad_maximum_fusion.refs_0_), channel_id=1, source_target_pairs={{0,1},{1,0},{2,3},{3,2},{4,5},{5,4},{6,7},{7,6},{8,9},{9,8},{10,11... | collective-permute-start | bytes 786440 | tf_op jit(solution)/shard_map/ppermute | solution.py:344
  47.5 12.2 %collective-permute-start.11 = (bf16[4,256,128]{2,1,0:T(8,128)(2,1)S(1)}, bf16[4,256,128]{2,1,0:T(8,128)(2,1)S(1)}, u32[]{:S(2)}, u32[]{:S(2)}) collective-permute-start(bf16[4,256,128]{2,1,0:T(8,128)(2,1)S(1)} %pad_maximum_fusion.refs_0_), channel_id=1, source_target_pairs={{0,2},{1,3},{2,0},{3,1},{4,6},{5,7},{6,4},{7,5},{8,10},{9,11},{10,... | collective-permute-start | bytes 786440 | tf_op jit(solution)/shard_map/ppermute | solution.py:344
  49.0 10.7 %collective-permute-start.12 = (bf16[4,256,128]{2,1,0:T(8,128)(2,1)S(1)}, bf16[4,256,128]{2,1,0:T(8,128)(2,1)S(1)}, u32[]{:S(2)}, u32[]{:S(2)}) collective-permute-start(bf16[4,256,128]{2,1,0:T(8,128)(2,1)S(1)} %pad_maximum_fusion.refs_0_), channel_id=1, source_target_pairs={{0,3},{1,2},{2,1},{3,0},{4,7},{5,6},{6,5},{7,4},{8,11},{9,10},{10,... | collective-permute-start | bytes 786440 | tf_op jit(solution)/shard_map/ppermute | solution.py:344
  61.5 1.1 copy-start
  62.6 91.8 %all-to-all-start = ((bf16[32,40,512]{2,1,0:T(8,128)(2,1)}), bf16[32,40,512]{2,1,0:T(8,128)(2,1)S(1)}, u32[]{:S(2)}, u32[]{:S(2)}) async-start(bf16[32,40,512]{2,1,0:T(8,128)(2,1)} %copy-done), calls=%async_computation | async-start | bytes 2621440 | tf_op jit(solution)/shard_map/all_to_all | solution.py:426
  67.2 87.2 %collective-permute-start.22 = (bf16[2048,256]{1,0:T(8,128)(2,1)}, bf16[2048,256]{1,0:T(8,128)(2,1)}, u32[]{:S(2)}, u32[]{:S(2)}) collective-permute-start(bf16[2048,256]{1,0:T(8,128)(2,1)} %get-tuple-element.39), channel_id=1, source_target_pairs={{0,3},{1,2},{2,1},{3,0},{4,7},{5,6},{6,5},{7,4},{8,11},{9,10},{10,... | collective-permute-start | bytes 3145736 | tf_op jit(solution)/shard_map/ppermute | solution.py:344
  69.9 50.7 %collective-permute-start.25 = (bf16[512,512]{1,0:T(8,128)(2,1)}, bf16[512,512]{1,0:T(8,128)(2,1)}, u32[]{:S(2)}, u32[]{:S(2)}) collective-permute-start(bf16[512,512]{1,0:T(8,128)(2,1)} %get-tuple-element.43), channel_id=1, source_target_pairs={{0,3},{1,2},{2,1},{3,0},{4,7},{5,6},{6,5},{7,4},{8,11},{9,10},{10,... | collective-permute-start | bytes 1572872 | tf_op jit(solution)/shard_map/ppermute | solution.py:344
  73.8 47.5 %copy-start.15 = (bf16[2048]{0:T(1024)(128)(2,1)S(1)}, bf16[2048]{0:T(1024)(128)(2,1)}, u32[]{:S(2)}) copy-start(bf16[2048]{0:T(1024)(128)(2,1)} %param.21) | copy-start | bytes 12292
  73.8 80.6 %collective-permute-start.20 = (bf16[2048,256]{1,0:T(8,128)(2,1)}, bf16[2048,256]{1,0:T(8,128)(2,1)}, u32[]{:S(2)}, u32[]{:S(2)}) collective-permute-start(bf16[2048,256]{1,0:T(8,128)(2,1)} %get-tuple-element.37), channel_id=1, source_target_pairs={{0,1},{1,0},{2,3},{3,2},{4,5},{5,4},{6,7},{7,6},{8,9},{9,8},{10,11... | collective-permute-start | bytes 3145736 | tf_op jit(solution)/shard_map/ppermute | solution.py:344
  75.6 78.8 %collective-permute-start.21 = (bf16[2048,256]{1,0:T(8,128)(2,1)}, bf16[2048,256]{1,0:T(8,128)(2,1)}, u32[]{:S(2)}, u32[]{:S(2)}) collective-permute-start(bf16[2048,256]{1,0:T(8,128)(2,1)} %get-tuple-element.38), channel_id=1, source_target_pairs={{0,2},{1,3},{2,0},{3,1},{4,6},{5,7},{6,4},{7,5},{8,10},{9,11},{10,... | collective-permute-start | bytes 3145736 | tf_op jit(solution)/shard_map/ppermute | solution.py:344
  79.6 73.2 %collective-permute-start.23 = (bf16[512,512]{1,0:T(8,128)(2,1)}, bf16[512,512]{1,0:T(8,128)(2,1)S(1)}, u32[]{:S(2)}, u32[]{:S(2)}) collective-permute-start(bf16[512,512]{1,0:T(8,128)(2,1)} %get-tuple-element.41), channel_id=1, source_target_pairs={{0,1},{1,0},{2,3},{3,2},{4,5},{5,4},{6,7},{7,6},{8,9},{9,8},{10,11... | collective-permute-start | bytes 1572872 | tf_op jit(solution)/shard_map/ppermute | solution.py:344
  120.6 33.0 %collective-permute-start.24 = (bf16[512,512]{1,0:T(8,128)(2,1)}, bf16[512,512]{1,0:T(8,128)(2,1)S(1)}, u32[]{:S(2)}, u32[]{:S(2)}) collective-permute-start(bf16[512,512]{1,0:T(8,128)(2,1)} %get-tuple-element.42), channel_id=1, source_target_pairs={{0,2},{1,3},{2,0},{3,1},{4,6},{5,7},{6,4},{7,5},{8,10},{9,11},{10,... | collective-permute-start | bytes 1572872 | tf_op jit(solution)/shard_map/ppermute | solution.py:344
  152.8 0.8 copy-start.8
  153.6 0.8 copy-start.10
  154.4 1.2 copy-start.2
  155.6 1.0 copy-start.7
  156.7 1.0 copy-start.9
  157.7 1.0 copy-start.11
  164.5 46.4 %all-to-all-start.1 = ((bf16[32,40,512]{2,1,0:T(8,128)(2,1)}), bf16[32,40,512]{2,1,0:T(8,128)(2,1)S(1)}, u32[]{:S(2)}, u32[]{:S(2)}) async-start(bf16[32,40,512]{2,1,0:T(8,128)(2,1)} %shard_map.152), calls=%async_computation.1 | async-start | bytes 2621440 | tf_op jit(solution)/shard_map/all_to_all | solution.py:439
  169.2 37.0 %copy-start.4 = (bf16[2048,128]{1,0:T(8,128)(2,1)S(1)}, bf16[2048,128]{1,0:T(8,128)(2,1)}, u32[]{:S(2)}) copy-start(bf16[2048,128]{1,0:T(8,128)(2,1)} %refs_6_.1) | copy-start | bytes 1572868
  169.2 37.0 %copy-start.5 = (bf16[2048,128]{1,0:T(8,128)(2,1)S(1)}, bf16[2048,128]{1,0:T(8,128)(2,1)}, u32[]{:S(2)}) copy-start(bf16[2048,128]{1,0:T(8,128)(2,1)} %refs_7_.1) | copy-start | bytes 1572868
  169.2 26.3 %collective-permute-start.14 = (bf16[512,512]{1,0:T(8,128)(2,1)S(1)}, bf16[512,512]{1,0:T(8,128)(2,1)S(1)}, u32[]{:S(2)}, u32[]{:S(2)}) collective-permute-start(bf16[512,512]{1,0:T(8,128)(2,1)S(1)} %get-tuple-element.34.refs_0_.mid_ref), channel_id=1, source_target_pairs={{0,2},{1,3},{2,0},{3,1},{4,6},{5,7},{6,4},{7,5},{8,10},{9,11},{10,... | collective-permute-start | bytes 1572872 | tf_op jit(solution)/shard_map/ppermute | solution.py:344
  171.1 26.5 %collective-permute-start.13 = (bf16[512,512]{1,0:T(8,128)(2,1)S(1)}, bf16[512,512]{1,0:T(8,128)(2,1)S(1)}, u32[]{:S(2)}, u32[]{:S(2)}) collective-permute-start(bf16[512,512]{1,0:T(8,128)(2,1)S(1)} %get-tuple-element.34.refs_0_.mid_ref), channel_id=1, source_target_pairs={{0,1},{1,0},{2,3},{3,2},{4,5},{5,4},{6,7},{7,6},{8,9},{9,8},{10,11... | collective-permute-start | bytes 1572872 | tf_op jit(solution)/shard_map/ppermute | solution.py:344
  195.6 8.8 %collective-permute-start.15 = (bf16[256,512]{1,0:T(8,128)(2,1)S(1)}, bf16[256,512]{1,0:T(8,128)(2,1)S(1)}, u32[]{:S(2)}, u32[]{:S(2)}) collective-permute-start(bf16[256,512]{1,0:T(8,128)(2,1)S(1)} %slice.8), channel_id=1, source_target_pairs={{0,1},{1,0},{2,3},{3,2},{4,5},{5,4},{6,7},{7,6},{8,9},{9,8},{10,11... | collective-permute-start | bytes 786440 | tf_op jit(solution)/shard_map/ppermute | solution.py:344
  197.6 8.6 %collective-permute-start.16 = (bf16[256,512]{1,0:T(8,128)(2,1)S(1)}, bf16[256,512]{1,0:T(8,128)(2,1)S(1)}, u32[]{:S(2)}, u32[]{:S(2)}) collective-permute-start(bf16[256,512]{1,0:T(8,128)(2,1)S(1)} %slice.9), channel_id=1, source_target_pairs={{0,2},{1,3},{2,0},{3,1},{4,6},{5,7},{6,4},{7,5},{8,10},{9,11},{10,... | collective-permute-start | bytes 786440 | tf_op jit(solution)/shard_map/ppermute | solution.py:344
  207.3 6.3 %collective-permute-start.17 = (bf16[512,128]{1,0:T(8,128)(2,1)S(1)}, bf16[512,128]{1,0:T(8,128)(2,1)S(1)}, u32[]{:S(2)}, u32[]{:S(2)}) collective-permute-start(bf16[512,128]{1,0:T(8,128)(2,1)S(1)} %shard_map.149.refs_0_), channel_id=1, source_target_pairs={{0,1},{1,0},{2,3},{3,2},{4,5},{5,4},{6,7},{7,6},{8,9},{9,8},{10,11... | collective-permute-start | bytes 393224 | tf_op jit(solution)/shard_map/ppermute | solution.py:344
  207.4 7.8 %collective-permute-start.18 = (bf16[512,128]{1,0:T(8,128)(2,1)S(1)}, bf16[512,128]{1,0:T(8,128)(2,1)S(1)}, u32[]{:S(2)}, u32[]{:S(2)}) collective-permute-start(bf16[512,128]{1,0:T(8,128)(2,1)S(1)} %shard_map.149.refs_0_), channel_id=1, source_target_pairs={{0,2},{1,3},{2,0},{3,1},{4,6},{5,7},{6,4},{7,5},{8,10},{9,11},{10,... | collective-permute-start | bytes 393224 | tf_op jit(solution)/shard_map/ppermute | solution.py:344
  207.8 7.3 %collective-permute-start.19 = (bf16[512,128]{1,0:T(8,128)(2,1)S(1)}, bf16[512,128]{1,0:T(8,128)(2,1)}, u32[]{:S(2)}, u32[]{:S(2)}) collective-permute-start(bf16[512,128]{1,0:T(8,128)(2,1)S(1)} %shard_map.149.refs_0_), channel_id=1, source_target_pairs={{0,3},{1,2},{2,1},{3,0},{4,7},{5,6},{6,5},{7,4},{8,11},{9,10},{10,... | collective-permute-start | bytes 393224 | tf_op jit(solution)/shard_map/ppermute | solution.py:344
  210.9 4.3 %copy-start.6 = (bf16[512,512]{1,0:T(8,128)(2,1)S(1)}, bf16[512,512]{1,0:T(8,128)(2,1)}, u32[]{:S(2)}) copy-start(bf16[512,512]{1,0:T(8,128)(2,1)} %refs_4_.3) | copy-start | bytes 1572868
